TPU v7x, 32 devices: a whole 2x2x4 slice. The times are simulated.
32 devices in a mesh: kv: 4 (over y, x), tp: 8 (over z, core).
Axes of the slice: x: 2, y: 2, z: 4, core: 2. Of those that a mesh axis runs over, the one named last changes fastest.
Arguments:
- tokens: bfloat16 [128, 4096], P(None, ('kv', 'tp')), may hold values from -41 to 41
- lengths: int32 [128], P('kv'), may hold values from 1 to 8192, 262144 in all
- retention_state: float32 [128, 16, 128, 256], P('kv', 'tp'), may hold values from -4 to 4
- mixer_gain: float32 [4096], P('kv'), may hold values from 0.1 to 1.9
- query_weight: bfloat16 [4096, 2048], P('kv', 'tp'), may hold values from -0.09375 to 0.09375
- key_weight: bfloat16 [4096, 2048], P('kv', 'tp'), may hold values from -0.09375 to 0.09375
- value_weight: bfloat16 [4096, 4096], P('kv', 'tp'), may hold values from -0.09375 to 0.09375
- gate_weight: bfloat16 [4096, 4096], P('kv', 'tp'), may hold values from -0.09375 to 0.09375
- output_weight: bfloat16 [4096, 4096], P('tp', 'kv'), may hold values from -0.125 to 0.125
- channel_gain: float32 [4096], P('kv'), may hold values from 0.1 to 1.9
- ffn_gate: bfloat16 [4096, 11264], P('kv', 'tp'), may hold values from -0.09375 to 0.09375
- ffn_up: bfloat16 [4096, 11264], P('kv', 'tp'), may hold values from -0.09375 to 0.09375
- ffn_down: bfloat16 [11264, 4096], P('tp', 'kv'), may hold values from -0.078125 to 0.078125
Outputs:
- layer_output: bfloat16 [128, 4096], P(None, ('kv', 'tp'))
- new_state: float32 [128, 16, 128, 256], P('kv', 'tp')
All inputs are finite; a program needn't handle non-finite values. No bound on the sum of `lengths` on one device may be relied on, other than what follows from the above.
Results may differ from a plain program's by a relative error of at most 0.022.
Values may be sent and summed in bfloat16 or wider, within the bound.
A program may use at most 64 MiB of HBM per device.

v0:
```python
import functools

import jax
import jax.numpy as jnp
import numpy as np
from jax import lax
from jax.experimental import pallas as pl
from jax.experimental.pallas import tpu as pltpu
from jax.sharding import PartitionSpec as P

D = 4096
HEADS = 16
QK = 128
LANES = 128


def rotate_heads(vectors, positions):
    half_dim = vectors.shape[-1] // 2
    frequency = 10000.0 ** (-jnp.arange(half_dim, dtype=jnp.float32) / half_dim)
    angles = positions.astype(jnp.float32)[:, None, None] * frequency
    cosine = jnp.cos(angles)
    sine_part = jnp.sin(angles)
    first_half = vectors[..., :half_dim]
    second = vectors[..., half_dim:]
    return jnp.concatenate(
        [first_half * cosine - second * sine_part, first_half * sine_part + second * cosine],
        axis=-1,
    )


def gathered_rows(columns):
    return lax.all_gather(columns, "tp", axis=1, tiled=True)


def owned_sums(partial_value, squares):
    raw_sums, totals = (
        lax.psum_scatter(
            partial_value.astype(jnp.bfloat16), "kv", scatter_dimension=0, tiled=True
        ).astype(jnp.float32),
        lax.psum_scatter(
            squares.astype(jnp.bfloat16), "kv", scatter_dimension=0, tiled=True
        ).astype(jnp.float32),
    )
    summed = raw_sums * lax.rsqrt(totals / D + 1e-06)[:, None]
    return summed


def every_sum(partial_value, squares):
    raw_sums, totals = (
        lax.psum(partial_value.astype(jnp.bfloat16), "kv").astype(jnp.float32),
        lax.psum(squares.astype(jnp.bfloat16), "kv").astype(jnp.float32),
    )
    summed = raw_sums * lax.rsqrt(totals / D + 1e-06)[:, None]
    return summed


def on_device(
    tokens,
    lengths,
    retention_state,
    mixer_gain,
    query_weight,
    key_weight,
    value_weight,
    gate_weight,
    output_weight,
    channel_gain,
    ffn_gate,
    ffn_up,
    ffn_down,
):
    feature_block = gathered_rows(tokens).astype(jnp.float32)
    squares = jnp.sum(feature_block * feature_block, axis=1)
    normed = (feature_block * mixer_gain).astype(jnp.bfloat16)
    partial_value = jnp.concatenate(
        [
            jnp.dot(normed, query_weight, preferred_element_type=jnp.float32),
            jnp.dot(normed, key_weight, preferred_element_type=jnp.float32),
            jnp.dot(normed, value_weight, preferred_element_type=jnp.float32),
            jnp.dot(normed, gate_weight, preferred_element_type=jnp.float32),
        ],
        axis=1,
    )
    owned_rows = owned_sums(partial_value, squares)
    local_heads = query_weight.shape[1] // QK
    q_width = query_weight.shape[1]
    v_width = value_weight.shape[1]
    head_width = v_width // local_heads
    seq_rows = owned_rows.shape[0]
    query_rows = rotate_heads(
        owned_rows[:, :q_width].reshape(seq_rows, local_heads, QK), lengths
    ).astype(jnp.bfloat16)
    key_rows = (
        rotate_heads(
            owned_rows[:, q_width : 2 * q_width].reshape(seq_rows, local_heads, QK), lengths
        )
        * QK ** (-0.5)
    ).astype(jnp.bfloat16)
    value_rows = (
        owned_rows[:, 2 * q_width : 2 * q_width + v_width]
        .astype(jnp.bfloat16)
        .reshape(seq_rows, local_heads, head_width)
    )
    gate_rows = owned_rows[:, 2 * q_width + v_width :]
    head_ids = (lax.axis_index("tp") * local_heads + jnp.arange(local_heads)).astype(jnp.float32)
    decay_rate = 1.0 - 2.0 ** (-5.0 - 10.0 * head_ids / (HEADS - 1))
    new_state = (
        decay_rate[None, :, None, None] * retention_state
        + key_rows.astype(jnp.float32)[..., :, None] * value_rows.astype(jnp.float32)[..., None, :]
    )
    retained = jnp.einsum(
        "bhk,bhkv->bhv", query_rows.astype(jnp.float32), new_state, precision=lax.Precision.HIGHEST
    )
    normalized = retained * lax.rsqrt(jnp.mean(retained * retained, axis=-1) + 1e-06)[..., None]
    merged = (normalized.reshape(seq_rows, v_width) * jax.nn.silu(gate_rows)).astype(jnp.bfloat16)
    mixed_part = jnp.dot(
        lax.all_gather(merged, "kv", axis=0, tiled=True),
        output_weight,
        preferred_element_type=jnp.float32,
    )
    mixed_cols = lax.psum_scatter(
        mixed_part.astype(jnp.bfloat16), "tp", scatter_dimension=1, tiled=True
    ).astype(jnp.float32)
    residual = (tokens.astype(jnp.float32) + mixed_cols).astype(jnp.bfloat16)
    block_two = gathered_rows(residual).astype(jnp.float32)
    squares_two = jnp.sum(block_two * block_two, axis=1)
    normed_two = (block_two * channel_gain).astype(jnp.bfloat16)
    partial_two = jnp.concatenate(
        [
            jnp.dot(normed_two, ffn_gate, preferred_element_type=jnp.float32),
            jnp.dot(normed_two, ffn_up, preferred_element_type=jnp.float32),
        ],
        axis=1,
    )
    hidden_units = ffn_gate.shape[1]
    summed = every_sum(partial_two, squares_two)
    hidden = (jax.nn.silu(summed[:, :hidden_units]) * summed[:, hidden_units:]).astype(jnp.bfloat16)
    down_part = jnp.dot(hidden, ffn_down, preferred_element_type=jnp.float32)
    down_sums = lax.psum_scatter(
        down_part.astype(jnp.bfloat16), "tp", scatter_dimension=1, tiled=True
    ).astype(jnp.float32)
    layer_output = (residual.astype(jnp.float32) + down_sums).astype(jnp.bfloat16)
    return (layer_output, new_state)


MESH_ID = pl.DeviceIdType.MESH
VMEM_TOTAL = 67043328
CORES = 2


def greet(groups):
    barrier = pltpu.get_barrier_semaphore()
    for axis, peers in groups:
        for peer in peers:
            pl.semaphore_signal(barrier, inc=1, device_id={axis: peer}, device_id_type=MESH_ID)
    pl.semaphore_wait(barrier, sum(len(peers) for _, peers in groups))


def send_all(axis, count, me, source, target, send_sems, recv_sems):
    copies = []
    for step in range(1, count):
        peer = lax.rem(me + step, count)
        copy = pltpu.make_async_remote_copy(
            src_ref=source(peer),
            dst_ref=target(step),
            send_sem=send_sems.at[step - 1],
            recv_sem=recv_sems.at[step - 1],
            device_id={axis: peer},
            device_id_type=MESH_ID,
        )
        copy.start()
        copies.append(copy)
    return copies


def received(copies):
    for copy in copies:
        copy.wait_recv()


def sent(copies):
    for copy in copies:
        copy.wait_send()


def load_all(pairs, sems):
    copies = [pltpu.make_async_copy(src, dst, sems.at[i]) for i, (src, dst) in enumerate(pairs)]
    for copy in copies:
        copy.start()
    return copies


def silu(value):
    return value / (1.0 + jnp.exp(-value))


def square_block(squares):
    head = squares.astype(jnp.bfloat16).astype(jnp.float32)
    rest = squares - head
    lane = lax.broadcasted_iota(jnp.int32, (squares.shape[0], LANES), 1)
    return jnp.where(lane < LANES // 2, head, rest).astype(jnp.bfloat16)


def square_total(block):
    return block[:, :1] + block[:, LANES // 2 : LANES // 2 + 1]


def wide(ref):
    return jnp.concatenate([ref[j] for j in range(ref.shape[0])], axis=1)


def remote(axis, peer, source, target, send_sem, recv_sem):
    return pltpu.make_async_remote_copy(
        src_ref=source, dst_ref=target, send_sem=send_sem, recv_sem=recv_sem,
        device_id={axis: peer}, device_id_type=MESH_ID,
    )


def gather_tp(slots, source, tp, n_tp, send_sems, recv_sems):
    chips = n_tp // CORES
    chip, core = tp // CORES, lax.rem(tp, CORES)
    partner = chip * CORES + 1 - core
    direct = []
    for step in range(1, chips):
        peer = lax.rem(chip + step, chips) * CORES + core
        direct.append(
            remote("tp", peer, source, slots.at[tp], send_sems.at[step], recv_sems.at[step])
        )
    across = [remote("tp", partner, source, slots.at[tp], send_sems.at[0], recv_sems.at[0])]
    for copy in direct + across:
        copy.start()

    def finish():
        for step in range(1, chips):
            direct[step - 1].wait_recv()
            slot = lax.rem(chip - step + chips, chips) * CORES + core
            i = chips - 1 + step
            copy = remote(
                "tp", partner, slots.at[slot], slots.at[slot], send_sems.at[i], recv_sems.at[i]
            )
            copy.start()
            across.append(copy)
        received(across)
        return direct + across

    return finish


def reduce_tp(lhs, weight, parts, swapped, staged, landed, tp, n_tp, send_sems, recv_sems):
    chips = n_tp // CORES
    chip, core = tp // CORES, lax.rem(tp, CORES)
    partner = chip * CORES + 1 - core
    columns = parts.shape[3]

    def multiply(side):
        starts = [pl.multiple_of((z * CORES + side) * columns, LANES) for z in range(chips)]
        rhs = jnp.concatenate([weight[:, pl.ds(start, columns)] for start in starts], axis=1)
        full = jnp.dot(lhs, rhs, preferred_element_type=jnp.float32).astype(jnp.bfloat16)
        for z in range(chips):
            parts[side, z] = full[:, z * columns : (z + 1) * columns]

    multiply(1 - core)
    swap = remote(
        "tp", partner, parts.at[1 - core], swapped, send_sems.at[0], recv_sems.at[0]
    )
    swap.start()
    multiply(core)
    swap.wait_recv()
    copies = []
    for step in range(1, chips):
        other = lax.rem(chip + step, chips)
        pair = parts[core, other].astype(jnp.float32) + swapped[other].astype(jnp.float32)
        staged[step - 1] = pair.astype(jnp.bfloat16)
        copy = remote(
            "tp", other * CORES + core, staged.at[step - 1], landed.at[step - 1],
            send_sems.at[step], recv_sems.at[step],
        )
        copy.start()
        copies.append(copy)
    total = parts[core, chip].astype(jnp.float32) + swapped[chip].astype(jnp.float32)
    for step in range(1, chips):
        copies[step - 1].wait_recv()
        total += landed[step - 1].astype(jnp.float32)
    return total, copies + [swap]


def total_of(own, landed):
    total = own.astype(jnp.float32)
    for step in range(landed.shape[0]):
        total += landed[step].astype(jnp.float32)
    return total


def layer_kernel(
    n_kv, n_tp, features,
    tokens_hbm, lengths_hbm, freq_hbm, gain_hbm, gain_two_hbm, state_hbm,
    wq_hbm, wk_hbm, wv_hbm, wg_hbm, wo_hbm, fg_hbm, fu_hbm, fd_hbm,
    out, state_out,
    state, lengths, freq, gain, gain_two, wq, wk, wv, wg, wo, fg, fu, fd,
    gathered, out_a, out_b, in_a, in_b, qk, value, retained, merged,
    parts_x, swapped_x, staged_x, landed_x, own, gathered_two,
    gate_out, up_out, gate_in, up_in, hidden, parts_d, swapped_d, staged_d, landed_d,
    load_sems, store_sem, gs, gr, as_, ar, bs, br, ms, mr, xs, xr, cs, cr, es, er, fs, fr, hs, hr, ds_, dr,
):
    kv, tp = lax.axis_index("kv"), lax.axis_index("tp")
    chips = n_tp // CORES
    chip, core = tp // CORES, lax.rem(tp, CORES)
    pairs = [
        (tokens_hbm, gathered.at[tp]), (lengths_hbm, lengths), (freq_hbm, freq), (gain_hbm, gain),
        (wq_hbm, wq), (wk_hbm, wk), (wv_hbm, wv), (wg_hbm, wg), (state_hbm, state),
        (gain_two_hbm, gain_two), (wo_hbm, wo), (fg_hbm, fg), (fu_hbm, fu), (fd_hbm, fd),
    ]
    loads = load_all(pairs, load_sems)
    along = [lax.rem(chip + step, chips) * CORES + core for step in range(1, chips)]
    greet([
        ("tp", along + [chip * CORES + 1 - core]),
        ("kv", [lax.rem(kv + step, n_kv) for step in range(1, n_kv)]),
    ])
    loads[0].wait()
    finish_g = gather_tp(gathered, gathered.at[tp], tp, n_tp, gs, gr)
    for i in (1, 2, 3):
        loads[i].wait()
    rows = out_a.shape[1]
    row = lax.broadcasted_iota(jnp.int32, (rows, rows), 0)
    col = lax.broadcasted_iota(jnp.int32, (rows, rows), 1)
    spread = jnp.where(row == col, lengths[...].astype(jnp.float32), 0.0)
    angles = jnp.sum(spread, axis=1, keepdims=True) * freq[...]
    cosine, sine = jnp.cos(angles), jnp.sin(angles)
    lane = lax.broadcasted_iota(jnp.int32, angles.shape, 1)
    sine = jnp.where(lane < QK // 2, -sine, sine)
    started = finish_g()

    def normalise(slots, gains):
        x = wide(slots).astype(jnp.float32)
        squares = jnp.sum(x * x, axis=1, keepdims=True)
        return (x * gains[...]).astype(jnp.bfloat16), square_block(squares).reshape(n_kv, rows, LANES)

    def project(lhs, weight):
        full = jnp.dot(lhs, weight[...], preferred_element_type=jnp.float32)
        return full.astype(jnp.bfloat16).reshape(n_kv, rows, full.shape[1])

    normed, squares = normalise(gathered, gain)
    q_width, v_width = wq.shape[1], wv.shape[1]
    heads = q_width // QK
    width = v_width // heads
    out_a[:, :, 2 * q_width :] = squares
    loads[4].wait()
    out_a[:, :, :q_width] = project(normed, wq)
    loads[5].wait()
    out_a[:, :, q_width : 2 * q_width] = project(normed, wk)
    first = send_all("kv", n_kv, kv, lambda p: out_a.at[p], lambda s: in_a.at[s - 1], as_, ar)
    loads[6].wait()
    out_b[:, :, :v_width] = project(normed, wv)
    loads[7].wait()
    out_b[:, :, v_width:] = project(normed, wg)
    second = send_all("kv", n_kv, kv, lambda p: out_b.at[p], lambda s: in_b.at[s - 1], bs, br)
    loads[8].wait()
    received(first)
    total = total_of(out_a[kv], in_a)
    scale = lax.rsqrt(square_total(total[:, 2 * q_width :]) / features + 1e-06)
    total = total * scale
    blocks = []
    for base, factor in ((0, 1.0), (q_width, QK ** (-0.5))):
        for head in range(heads):
            part = total[:, base + head * QK : base + (head + 1) * QK]
            turned = (part * cosine + pltpu.roll(part, QK // 2, 1) * sine) * factor
            blocks.append(turned.astype(jnp.bfloat16).astype(jnp.float32))
    qk[...] = jnp.concatenate(blocks, axis=0).T
    block = 4

    def turned_to(start):
        return pltpu.roll(qk[...], lax.rem(LANES - start, LANES), 1)

    def query_step(i, carry):
        start = i * block
        turned = turned_to(start)
        for s in range(block):
            for head in range(heads):
                query = turned[:, head * rows + s : head * rows + s + 1]
                retained[pl.ds(start + s, 1), head * width : (head + 1) * width] = jnp.sum(
                    query * state[start + s, head], axis=0, keepdims=True
                )
        return carry

    lax.fori_loop(0, rows // block, query_step, 0)
    decays = []
    for head in range(heads):
        number = jnp.full((1, width), tp * heads + head, jnp.int32).astype(jnp.float32)
        decays.append(1.0 - jnp.exp2(-5.0 - 10.0 * number / (heads * n_tp - 1)))
    received(second)
    total = total_of(out_b[kv], in_b) * scale
    value[...] = total[:, :v_width].astype(jnp.bfloat16).astype(jnp.float32)
    pieces = []
    for head in range(heads):
        overlap = jnp.sum(blocks[head] * blocks[heads + head], axis=1, keepdims=True)
        span = slice(head * width, (head + 1) * width)
        piece = decays[head] * retained[:, span] + overlap * value[:, span]
        pieces.append(piece * lax.rsqrt(jnp.mean(piece * piece, axis=1, keepdims=True) + 1e-06))
    merged[kv] = (jnp.concatenate(pieces, axis=1) * silu(total[:, v_width:])).astype(jnp.bfloat16)
    copies_m = send_all("kv", n_kv, kv, lambda p: merged.at[kv], lambda s: merged.at[kv], ms, mr)

    def update_step(i, carry):
        start = i * block
        turned = turned_to(start)
        for s in range(block):
            for head in range(heads):
                lane = (heads + head) * rows + s
                outer = turned[:, lane : lane + 1] * value[pl.ds(start + s, 1), head * width : (head + 1) * width]
                state[start + s, head] = decays[head] * state[start + s, head] + outer
        return carry

    lax.fori_loop(0, rows // block, update_step, 0)
    loads[10].wait()
    received(copies_m)
    store = pltpu.make_async_copy(state, state_out, store_sem)
    store.start()
    batch = n_kv * rows
    total, copies_x = reduce_tp(
        merged[...].reshape(batch, v_width), wo, parts_x, swapped_x, staged_x, landed_x, tp, n_tp, xs, xr
    )
    residual = (tokens_of(gathered, tp) + total).astype(jnp.bfloat16)
    own[...] = residual
    gathered_two[tp] = residual
    finish_c = gather_tp(gathered_two, own, tp, n_tp, cs, cr)
    loads[9].wait()
    loads[11].wait()
    copies_c = finish_c()
    normed, squares = normalise(gathered_two, gain_two)
    units = fg.shape[1]
    gate_out[:, :, units:] = squares
    gate_out[:, :, :units] = project(normed, fg)
    copies_e = send_all("kv", n_kv, kv, lambda p: gate_out.at[p], lambda s: gate_in.at[s - 1], es, er)
    loads[12].wait()
    up_out[...] = project(normed, fu)
    copies_f = send_all("kv", n_kv, kv, lambda p: up_out.at[p], lambda s: up_in.at[s - 1], fs, fr)
    received(copies_e)
    total = total_of(gate_out[kv], gate_in)
    scale = lax.rsqrt(square_total(total[:, units:]) / features + 1e-06)
    activated = silu(total[:, :units] * scale)
    received(copies_f)
    hidden[kv] = (activated * (total_of(up_out[kv], up_in) * scale)).astype(jnp.bfloat16)
    copies_h = send_all("kv", n_kv, kv, lambda p: hidden.at[kv], lambda s: hidden.at[kv], hs, hr)
    loads[13].wait()
    received(copies_h)
    total, copies_d = reduce_tp(
        hidden[...].reshape(batch, units), fd, parts_d, swapped_d, staged_d, landed_d, tp, n_tp, ds_, dr
    )
    out[...] = (own[...].astype(jnp.float32) + total).astype(jnp.bfloat16)
    for copies in (started, first, second, copies_m, copies_x, copies_c, copies_e, copies_f, copies_h, copies_d):
        sent(copies)
    store.wait()


def finish_kernel(state, out, state_to, out_to, slots, small, load_sems, store_sems):
    chunks, size = slots.shape[0], slots.shape[1]
    pairs, targets = [(out, small)], [(small, out_to)]
    for i in range(chunks):
        pairs.append((state.at[pl.ds(i * size, size)], slots.at[i]))
        targets.append((slots.at[i], state_to.at[pl.ds(i * size, size)]))
    loads = load_all(pairs, load_sems)
    stores = []
    for i, (source, target) in enumerate(targets):
        loads[i].wait()
        copy = pltpu.make_async_copy(source, target, store_sems.at[i])
        copy.start()
        stores.append(copy)
    for copy in stores:
        copy.wait()


def tokens_of(slots, tp):
    return slots[tp].astype(jnp.float32)


def fused_on_device(n_kv, n_tp, *arrays):
    (
        tokens, lengths, state, mixer_gain, wq, wk, wv, wg, wo, channel_gain, fg, fu, fd,
    ) = arrays
    batch, columns = tokens.shape
    rows = state.shape[0]
    depth, q_width = wq.shape
    v_width, units = wv.shape[1], fg.shape[1]
    bf16, f32 = jnp.bfloat16, jnp.float32
    vmem = pl.BlockSpec(memory_space=pltpu.VMEM)
    hbm = pl.BlockSpec(memory_space=pltpu.HBM)
    dma = pltpu.SemaphoreType.DMA
    tp_sems, kv_sems = [dma((n_tp - 1,))] * 2, [dma((n_kv - 1,))] * 2
    chips = n_tp // CORES
    chip_sems = [dma((chips,))] * 2
    index = np.arange(QK) % (QK // 2)
    freq = jnp.asarray((10000.0 ** (-index / (QK // 2))).astype(np.float32))[None, :]
    a_width, b_width = 2 * q_width + LANES, 2 * v_width
    reduce_scratch = [
        pltpu.VMEM((CORES, chips, batch, columns), bf16),
        pltpu.VMEM((chips, batch, columns), bf16),
        pltpu.VMEM((chips - 1, batch, columns), bf16),
        pltpu.VMEM((chips - 1, batch, columns), bf16),
    ]
    out, new_state = pl.pallas_call(
        functools.partial(layer_kernel, n_kv, n_tp, depth * n_kv),
        out_shape=(
            jax.ShapeDtypeStruct(tokens.shape, bf16),
            jax.ShapeDtypeStruct(state.shape, f32),
        ),
        in_specs=[hbm] * 14,
        out_specs=(vmem, hbm),
        scratch_shapes=[
            pltpu.VMEM(state.shape, f32),
            pltpu.VMEM((1, rows), jnp.int32),
            pltpu.VMEM((1, QK), f32),
            pltpu.VMEM((1, depth), f32),
            pltpu.VMEM((1, depth), f32),
        ]
        + [pltpu.VMEM(w.shape, bf16) for w in (wq, wk, wv, wg, wo, fg, fu, fd)]
        + [
            pltpu.VMEM((n_tp, batch, columns), bf16),
            pltpu.VMEM((n_kv, rows, a_width), bf16),
            pltpu.VMEM((n_kv, rows, b_width), bf16),
            pltpu.VMEM((n_kv - 1, rows, a_width), bf16),
            pltpu.VMEM((n_kv - 1, rows, b_width), bf16),
            pltpu.VMEM((QK, LANES), f32),
            pltpu.VMEM((rows, v_width), f32),
            pltpu.VMEM((rows, v_width), f32),
            pltpu.VMEM((n_kv, rows, v_width), bf16),
        ]
        + reduce_scratch
        + [
            pltpu.VMEM((batch, columns), bf16),
            pltpu.VMEM((n_tp, batch, columns), bf16),
            pltpu.VMEM((n_kv, rows, units + LANES), bf16),
            pltpu.VMEM((n_kv, rows, units), bf16),
            pltpu.VMEM((n_kv - 1, rows, units + LANES), bf16),
            pltpu.VMEM((n_kv - 1, rows, units), bf16),
            pltpu.VMEM((n_kv, rows, units), bf16),
        ]
        + reduce_scratch
        + [dma((14,)), dma]
        + tp_sems + kv_sems + kv_sems + kv_sems + chip_sems + tp_sems + kv_sems + kv_sems + kv_sems + chip_sems,
        compiler_params=pltpu.CompilerParams(
            collective_id=0, has_side_effects=True, vmem_limit_bytes=VMEM_TOTAL
        ),
        name="layer",
    )(tokens, lengths[None, :], freq, mixer_gain[None, :], channel_gain[None, :], state, wq, wk, wv, wg, wo, fg, fu, fd)
    chunks = 8
    new_state, out = pl.pallas_call(
        finish_kernel,
        out_shape=(
            jax.ShapeDtypeStruct(state.shape, f32),
            jax.ShapeDtypeStruct(tokens.shape, bf16),
        ),
        in_specs=[hbm, hbm],
        out_specs=(hbm, hbm),
        scratch_shapes=[
            pltpu.VMEM((chunks, rows // chunks) + state.shape[1:], f32),
            pltpu.VMEM(tokens.shape, bf16),
            dma((chunks + 1,)),
            dma((chunks + 1,)),
        ],
        compiler_params=pltpu.CompilerParams(vmem_limit_bytes=VMEM_TOTAL),
        name="finish",
    )(new_state, out)
    return out, new_state


def fits(n_kv, n_tp, arrays):
    tokens, state, ffn_gate = arrays[0], arrays[2], arrays[10]
    rows, heads = state.shape[0], state.shape[1]
    return (
        tokens.shape[1] % LANES == 0
        and n_tp % CORES == 0
        and n_tp > CORES
        and n_kv > 1
        and 4 * state.size < VMEM_TOTAL // 4
        and ffn_gate.shape[1] % LANES == 0
        and rows % 16 == 0
        and 2 * heads * rows == LANES
        and state.shape[2] == QK == LANES
        and state.shape[3] % LANES == 0
    )


def per_device(n_kv, n_tp, *arrays):
    if fits(n_kv, n_tp, arrays):
        return fused_on_device(n_kv, n_tp, *arrays)
    return on_device(*arrays)


def solution(mesh):
    in_specs = (
        P(None, ("kv", "tp")),
        P("kv"),
        P("kv", "tp", None, None),
        P("kv"),
        P("kv", "tp"),
        P("kv", "tp"),
        P("kv", "tp"),
        P("kv", "tp"),
        P("tp", "kv"),
        P("kv"),
        P("kv", "tp"),
        P("kv", "tp"),
        P("tp", "kv"),
    )
    out_specs = (P(None, ("kv", "tp")), P("kv", "tp", None, None))
    return jax.shard_map(
        functools.partial(per_device, mesh.shape["kv"], mesh.shape["tp"]),
        mesh=mesh, in_specs=in_specs, out_specs=out_specs, check_vma=False
    )
```

profile of v0, /device:TPU:0, one launch (start us, length us, event | category | flops | bytes accessed | tf_op | source)
XLA Modules:
  0.0 64.5 jit_solution(7229478742108584692)
XLA Ops:
  0.6 57.4 %layer.1 = (bf16[128,128]{1,0:T(8,128)(2,1)}, f32[32,2,128,256]{3,2,1,0:T(8,128)}) custom-call(bf16[128,128]{1,0:T(8,128)(2,1)} %tokens_hbm.1, s32[1,32]{1,0:T(1,128)} %bitcast.5, f32[1,128]{1,0:T(1,128)} %constant.4.freq_hbm, f32[1,1024]{1,0:T(1,128)} %bitcast.3, f32[1,1024]{1,0:T(1,128)} %bitcast.4, f32[32,2,128,256]{3,2,1,0:T(8,128)} %state_hbm.1, ...), custom_call_target="tpu_custom_call" | custom-call | tf_op jit(solution)/shard_map/layer/pallas_call | solution.py:499
  58.0 6.5 %finish.1 = (f32[32,2,128,256]{3,2,1,0:T(8,128)}, bf16[128,128]{1,0:T(8,128)(2,1)}) custom-call(f32[32,2,128,256]{3,2,1,0:T(8,128)} %get-tuple-element.6.state, bf16[128,128]{1,0:T(8,128)(2,1)} %get-tuple-element.7.out), custom_call_target="tpu_custom_call" | custom-call | tf_op jit(solution)/shard_map/finish/pallas_call | solution.py:545
where the time goes:
time: 64.6 us; the launch traced here: 64.5 us
  Pallas kernels  63.8 us (99%)
    pallas_call x1, Pallas kernels, fused_on_device(): pl.pallas_call(functools.partial(layer_kernel, n_kv, n_tp, depth * n_kv),...  57.4 us
    pallas_call x1, Pallas kernels, fused_on_device(): pl.pallas_call(finish_kernel, out_shape=(jax.ShapeDtypeStruct(state.shape...  6.47 us

commit v1 on v0

--- a/solution.py
+++ b/solution.py
@@ -295,12 +295,12 @@
     n_kv, n_tp, features,
     tokens_hbm, lengths_hbm, freq_hbm, gain_hbm, gain_two_hbm, state_hbm,
     wq_hbm, wk_hbm, wv_hbm, wg_hbm, wo_hbm, fg_hbm, fu_hbm, fd_hbm,
-    out, state_out,
-    state, lengths, freq, gain, gain_two, wq, wk, wv, wg, wo, fg, fu, fd,
+    out, state,
+    lengths, freq, gain, gain_two, wq, wk, wv, wg, wo, fg, fu, fd,
     gathered, out_a, out_b, in_a, in_b, qk, value, retained, merged,
     parts_x, swapped_x, staged_x, landed_x, own, gathered_two,
     gate_out, up_out, gate_in, up_in, hidden, parts_d, swapped_d, staged_d, landed_d,
-    load_sems, store_sem, gs, gr, as_, ar, bs, br, ms, mr, xs, xr, cs, cr, es, er, fs, fr, hs, hr, ds_, dr,
+    load_sems, gs, gr, as_, ar, bs, br, ms, mr, xs, xr, cs, cr, es, er, fs, fr, hs, hr, ds_, dr,
 ):
     kv, tp = lax.axis_index("kv"), lax.axis_index("tp")
     chips = n_tp // CORES
@@ -412,8 +412,6 @@
     lax.fori_loop(0, rows // block, update_step, 0)
     loads[10].wait()
     received(copies_m)
-    store = pltpu.make_async_copy(state, state_out, store_sem)
-    store.start()
     batch = n_kv * rows
     total, copies_x = reduce_tp(
         merged[...].reshape(batch, v_width), wo, parts_x, swapped_x, staged_x, landed_x, tp, n_tp, xs, xr
@@ -448,23 +446,16 @@
     out[...] = (own[...].astype(jnp.float32) + total).astype(jnp.bfloat16)
     for copies in (started, first, second, copies_m, copies_x, copies_c, copies_e, copies_f, copies_h, copies_d):
         sent(copies)
-    store.wait()
-
-
-def finish_kernel(state, out, state_to, out_to, slots, small, load_sems, store_sems):
-    chunks, size = slots.shape[0], slots.shape[1]
-    pairs, targets = [(out, small)], [(small, out_to)]
+
+
+def finish_kernel(state, out, state_to, out_to, store_sems):
+    chunks = store_sems.shape[0] - 1
+    size = state.shape[0] // chunks
+    targets = [(out, out_to)]
     for i in range(chunks):
-        pairs.append((state.at[pl.ds(i * size, size)], slots.at[i]))
-        targets.append((slots.at[i], state_to.at[pl.ds(i * size, size)]))
-    loads = load_all(pairs, load_sems)
-    stores = []
-    for i, (source, target) in enumerate(targets):
-        loads[i].wait()
-        copy = pltpu.make_async_copy(source, target, store_sems.at[i])
-        copy.start()
-        stores.append(copy)
-    for copy in stores:
+        part = pl.ds(i * size, size)
+        targets.append((state.at[part], state_to.at[part]))
+    for copy in load_all(targets, store_sems):
         copy.wait()
 
 
@@ -499,13 +490,12 @@
     out, new_state = pl.pallas_call(
         functools.partial(layer_kernel, n_kv, n_tp, depth * n_kv),
         out_shape=(
-            jax.ShapeDtypeStruct(tokens.shape, bf16),
-            jax.ShapeDtypeStruct(state.shape, f32),
+            pltpu.VMEM(tokens.shape, bf16),
+            pltpu.VMEM(state.shape, f32),
         ),
         in_specs=[hbm] * 14,
-        out_specs=(vmem, hbm),
+        out_specs=(vmem, vmem),
         scratch_shapes=[
-            pltpu.VMEM(state.shape, f32),
             pltpu.VMEM((1, rows), jnp.int32),
             pltpu.VMEM((1, QK), f32),
             pltpu.VMEM((1, depth), f32),
@@ -534,29 +524,23 @@
             pltpu.VMEM((n_kv, rows, units), bf16),
         ]
         + reduce_scratch
-        + [dma((14,)), dma]
+        + [dma((14,))]
         + tp_sems + kv_sems + kv_sems + kv_sems + chip_sems + tp_sems + kv_sems + kv_sems + kv_sems + chip_sems,
         compiler_params=pltpu.CompilerParams(
-            collective_id=0, has_side_effects=True, vmem_limit_bytes=VMEM_TOTAL
+            collective_id=0, has_side_effects=True, vmem_limit_bytes=40000000
         ),
         name="layer",
-    )(tokens, lengths[None, :], freq, mixer_gain[None, :], channel_gain[None, :], state, wq, wk, wv, wg, wo, fg, fu, fd)
-    chunks = 8
+    )(*[pltpu.with_memory_space_constraint(a, pltpu.HBM) for a in (tokens, lengths[None, :], freq, mixer_gain[None, :], channel_gain[None, :], state, wq, wk, wv, wg, wo, fg, fu, fd)])
     new_state, out = pl.pallas_call(
         finish_kernel,
         out_shape=(
             jax.ShapeDtypeStruct(state.shape, f32),
             jax.ShapeDtypeStruct(tokens.shape, bf16),
         ),
-        in_specs=[hbm, hbm],
+        in_specs=[vmem, vmem],
         out_specs=(hbm, hbm),
-        scratch_shapes=[
-            pltpu.VMEM((chunks, rows // chunks) + state.shape[1:], f32),
-            pltpu.VMEM(tokens.shape, bf16),
-            dma((chunks + 1,)),
-            dma((chunks + 1,)),
-        ],
-        compiler_params=pltpu.CompilerParams(vmem_limit_bytes=VMEM_TOTAL),
+        scratch_shapes=[dma((9,))],
+        compiler_params=pltpu.CompilerParams(vmem_limit_bytes=20000000),
         name="finish",
     )(new_state, out)
     return out, new_state

time: 64.6 us -> 60.9 us (0.943)
  Pallas kernels: 63.8 us -> 60.1 us
    pallas_call x1, Pallas kernels: 6.47 us -> 3.39 us  [fused_on_device(): pl.pallas_call(finish_kernel, out_shape=(jax.ShapeDtypeStruct(state.shape...]
where the time goes in v1:
time: 60.9 us; the launch traced here: 60.8 us
  Pallas kernels  60.1 us (99%)
  between operations  0.64 us (1%)
    pallas_call x1, Pallas kernels, fused_on_device(): pl.pallas_call(functools.partial(layer_kernel, n_kv, n_tp, depth * n_kv),...  56.7 us
    pallas_call x1, Pallas kernels, fused_on_device(): pl.pallas_call(finish_kernel, out_shape=(jax.ShapeDtypeStruct(state.shape...  3.39 us

profile of v1, /device:TPU:0, one launch (start us, length us, event | category | flops | bytes accessed | tf_op | source)
XLA Modules:
  0.0 60.8 jit_solution(17926149004079323494)
XLA Ops:
  0.6 56.7 %layer.1 = (bf16[128,128]{1,0:T(8,128)(2,1)S(1)}, f32[32,2,128,256]{3,2,1,0:T(8,128)S(1)}) custom-call(bf16[128,128]{1,0:T(8,128)(2,1)} %tokens_hbm.1, s32[1,32]{1,0:T(1,128)} %bitcast.5, f32[1,128]{1,0:T(1,128)} %constant.4.freq_hbm, f32[1,1024]{1,0:T(1,128)} %bitcast.3, f32[1,1024]{1,0:T(1,128)} %bitcast.4, f32[32,2,128,256]{3,2,1,0:T(8,128)} %state_hbm.1, ...), custom_call_target="tpu_custom_call" | custom-call | tf_op jit(solution)/shard_map/layer/pallas_call | solution.py:490
  57.4 3.4 %finish.1 = (f32[32,2,128,256]{3,2,1,0:T(8,128)}, bf16[128,128]{1,0:T(8,128)(2,1)}) custom-call(f32[32,2,128,256]{3,2,1,0:T(8,128)S(1)} %get-tuple-element.6.state, bf16[128,128]{1,0:T(8,128)(2,1)S(1)} %get-tuple-element.7.out), custom_call_target="tpu_custom_call" | custom-call | tf_op jit(solution)/shard_map/finish/pallas_call | solution.py:534

commit v2 on v1

v2 whole, which is shorter than its diff:
```python
import functools

import jax
import jax.numpy as jnp
import numpy as np
from jax import lax
from jax.experimental import pallas as pl
from jax.experimental.pallas import tpu as pltpu
from jax.sharding import PartitionSpec as P

D = 4096
HEADS = 16
QK = 128
LANES = 128


def rotate_heads(vectors, positions):
    half_dim = vectors.shape[-1] // 2
    frequency = 10000.0 ** (-jnp.arange(half_dim, dtype=jnp.float32) / half_dim)
    angles = positions.astype(jnp.float32)[:, None, None] * frequency
    cosine = jnp.cos(angles)
    sine_part = jnp.sin(angles)
    first_half = vectors[..., :half_dim]
    second = vectors[..., half_dim:]
    return jnp.concatenate(
        [first_half * cosine - second * sine_part, first_half * sine_part + second * cosine],
        axis=-1,
    )


def gathered_rows(columns):
    return lax.all_gather(columns, "tp", axis=1, tiled=True)


def owned_sums(partial_value, squares):
    raw_sums, totals = (
        lax.psum_scatter(
            partial_value.astype(jnp.bfloat16), "kv", scatter_dimension=0, tiled=True
        ).astype(jnp.float32),
        lax.psum_scatter(
            squares.astype(jnp.bfloat16), "kv", scatter_dimension=0, tiled=True
        ).astype(jnp.float32),
    )
    summed = raw_sums * lax.rsqrt(totals / D + 1e-06)[:, None]
    return summed


def every_sum(partial_value, squares):
    raw_sums, totals = (
        lax.psum(partial_value.astype(jnp.bfloat16), "kv").astype(jnp.float32),
        lax.psum(squares.astype(jnp.bfloat16), "kv").astype(jnp.float32),
    )
    summed = raw_sums * lax.rsqrt(totals / D + 1e-06)[:, None]
    return summed


def on_device(
    tokens,
    lengths,
    retention_state,
    mixer_gain,
    query_weight,
    key_weight,
    value_weight,
    gate_weight,
    output_weight,
    channel_gain,
    ffn_gate,
    ffn_up,
    ffn_down,
):
    feature_block = gathered_rows(tokens).astype(jnp.float32)
    squares = jnp.sum(feature_block * feature_block, axis=1)
    normed = (feature_block * mixer_gain).astype(jnp.bfloat16)
    partial_value = jnp.concatenate(
        [
            jnp.dot(normed, query_weight, preferred_element_type=jnp.float32),
            jnp.dot(normed, key_weight, preferred_element_type=jnp.float32),
            jnp.dot(normed, value_weight, preferred_element_type=jnp.float32),
            jnp.dot(normed, gate_weight, preferred_element_type=jnp.float32),
        ],
        axis=1,
    )
    owned_rows = owned_sums(partial_value, squares)
    local_heads = query_weight.shape[1] // QK
    q_width = query_weight.shape[1]
    v_width = value_weight.shape[1]
    head_width = v_width // local_heads
    seq_rows = owned_rows.shape[0]
    query_rows = rotate_heads(
        owned_rows[:, :q_width].reshape(seq_rows, local_heads, QK), lengths
    ).astype(jnp.bfloat16)
    key_rows = (
        rotate_heads(
            owned_rows[:, q_width : 2 * q_width].reshape(seq_rows, local_heads, QK), lengths
        )
        * QK ** (-0.5)
    ).astype(jnp.bfloat16)
    value_rows = (
        owned_rows[:, 2 * q_width : 2 * q_width + v_width]
        .astype(jnp.bfloat16)
        .reshape(seq_rows, local_heads, head_width)
    )
    gate_rows = owned_rows[:, 2 * q_width + v_width :]
    head_ids = (lax.axis_index("tp") * local_heads + jnp.arange(local_heads)).astype(jnp.float32)
    decay_rate = 1.0 - 2.0 ** (-5.0 - 10.0 * head_ids / (HEADS - 1))
    new_state = (
        decay_rate[None, :, None, None] * retention_state
        + key_rows.astype(jnp.float32)[..., :, None] * value_rows.astype(jnp.float32)[..., None, :]
    )
    retained = jnp.einsum(
        "bhk,bhkv->bhv", query_rows.astype(jnp.float32), new_state, precision=lax.Precision.HIGHEST
    )
    normalized = retained * lax.rsqrt(jnp.mean(retained * retained, axis=-1) + 1e-06)[..., None]
    merged = (normalized.reshape(seq_rows, v_width) * jax.nn.silu(gate_rows)).astype(jnp.bfloat16)
    mixed_part = jnp.dot(
        lax.all_gather(merged, "kv", axis=0, tiled=True),
        output_weight,
        preferred_element_type=jnp.float32,
    )
    mixed_cols = lax.psum_scatter(
        mixed_part.astype(jnp.bfloat16), "tp", scatter_dimension=1, tiled=True
    ).astype(jnp.float32)
    residual = (tokens.astype(jnp.float32) + mixed_cols).astype(jnp.bfloat16)
    block_two = gathered_rows(residual).astype(jnp.float32)
    squares_two = jnp.sum(block_two * block_two, axis=1)
    normed_two = (block_two * channel_gain).astype(jnp.bfloat16)
    partial_two = jnp.concatenate(
        [
            jnp.dot(normed_two, ffn_gate, preferred_element_type=jnp.float32),
            jnp.dot(normed_two, ffn_up, preferred_element_type=jnp.float32),
        ],
        axis=1,
    )
    hidden_units = ffn_gate.shape[1]
    summed = every_sum(partial_two, squares_two)
    hidden = (jax.nn.silu(summed[:, :hidden_units]) * summed[:, hidden_units:]).astype(jnp.bfloat16)
    down_part = jnp.dot(hidden, ffn_down, preferred_element_type=jnp.float32)
    down_sums = lax.psum_scatter(
        down_part.astype(jnp.bfloat16), "tp", scatter_dimension=1, tiled=True
    ).astype(jnp.float32)
    layer_output = (residual.astype(jnp.float32) + down_sums).astype(jnp.bfloat16)
    return (layer_output, new_state)


MESH_ID = pl.DeviceIdType.MESH
VMEM_TOTAL = 67043328
CORES = 2
LAYER_VMEM = 50000000
FINISH_VMEM = 20000000


def greet(groups):
    barrier = pltpu.get_barrier_semaphore()
    for axis, peers in groups:
        for peer in peers:
            pl.semaphore_signal(barrier, inc=1, device_id={axis: peer}, device_id_type=MESH_ID)
    pl.semaphore_wait(barrier, sum(len(peers) for _, peers in groups))


def send_all(axis, count, me, source, target, send_sems, recv_sems):
    copies = []
    for step in range(1, count):
        peer = lax.rem(me + step, count)
        copy = pltpu.make_async_remote_copy(
            src_ref=source(peer),
            dst_ref=target(step),
            send_sem=send_sems.at[step - 1],
            recv_sem=recv_sems.at[step - 1],
            device_id={axis: peer},
            device_id_type=MESH_ID,
        )
        copy.start()
        copies.append(copy)
    return copies


def received(copies):
    for copy in copies:
        copy.wait_recv()


def sent(copies):
    for copy in copies:
        copy.wait_send()


def load_all(pairs, sems):
    copies = [pltpu.make_async_copy(src, dst, sems.at[i]) for i, (src, dst) in enumerate(pairs)]
    for copy in copies:
        copy.start()
    return copies


def silu(value):
    return value / (1.0 + jnp.exp(-value))


def square_block(squares):
    head = squares.astype(jnp.bfloat16).astype(jnp.float32)
    rest = squares - head
    lane = lax.broadcasted_iota(jnp.int32, (squares.shape[0], LANES), 1)
    return jnp.where(lane < LANES // 2, head, rest).astype(jnp.bfloat16)


def square_total(block):
    return block[:, :1] + block[:, LANES // 2 : LANES // 2 + 1]


def remote(axis, peer, source, target, send_sem, recv_sem):
    return pltpu.make_async_remote_copy(
        src_ref=source, dst_ref=target, send_sem=send_sem, recv_sem=recv_sem,
        device_id={axis: peer}, device_id_type=MESH_ID,
    )


def start_gather(slots, tp, n_tp, send_sems, recv_sems):
    chips = n_tp // CORES
    chip, core = tp // CORES, lax.rem(tp, CORES)
    partner = chip * CORES + 1 - core
    direct = []
    for step in range(1, chips):
        peer = lax.rem(chip + step, chips) * CORES + core
        direct.append(
            remote("tp", peer, slots.at[tp], slots.at[tp], send_sems.at[step], recv_sems.at[step])
        )
    across = [remote("tp", partner, slots.at[tp], slots.at[tp], send_sems.at[0], recv_sems.at[0])]
    for copy in direct + across:
        copy.start()

    def relay():
        for step in range(1, chips):
            direct[step - 1].wait_recv()
            slot = lax.rem(chip - step + chips, chips) * CORES + core
            i = chips - 1 + step
            copy = remote(
                "tp", partner, slots.at[slot], slots.at[slot], send_sems.at[i], recv_sems.at[i]
            )
            copy.start()
            across.append(copy)

    def finish():
        received(across)
        return direct + across

    return relay, finish


def start_reduce(lhs, weight, parts, swapped, tp, n_tp, send_sems, recv_sems):
    chips = n_tp // CORES
    chip, core = tp // CORES, lax.rem(tp, CORES)
    columns = parts.shape[3]

    def multiply(side):
        starts = [pl.multiple_of((z * CORES + side) * columns, LANES) for z in range(chips)]
        rhs = jnp.concatenate([weight[:, pl.ds(start, columns)] for start in starts], axis=1)
        full = jnp.dot(lhs, rhs, preferred_element_type=jnp.float32).astype(jnp.bfloat16)
        for z in range(chips):
            parts[side, z] = full[:, z * columns : (z + 1) * columns]

    multiply(1 - core)
    swap = remote(
        "tp", chip * CORES + 1 - core, parts.at[1 - core], swapped, send_sems.at[0], recv_sems.at[0]
    )
    swap.start()
    multiply(core)
    return swap


def spread_pairs(swap, parts, swapped, staged, landed, tp, n_tp, send_sems, recv_sems):
    chips = n_tp // CORES
    chip, core = tp // CORES, lax.rem(tp, CORES)
    swap.wait_recv()
    copies = []
    for step in range(1, chips):
        other = lax.rem(chip + step, chips)
        pair = parts[core, other].astype(jnp.float32) + swapped[other].astype(jnp.float32)
        staged[step - 1] = pair.astype(jnp.bfloat16)
        copy = remote(
            "tp", other * CORES + core, staged.at[step - 1], landed.at[step - 1],
            send_sems.at[step], recv_sems.at[step],
        )
        copy.start()
        copies.append(copy)
    return copies


def pairs_total(copies, parts, swapped, landed, tp):
    chip, core = tp // CORES, lax.rem(tp, CORES)
    total = parts[core, chip].astype(jnp.float32) + swapped[chip].astype(jnp.float32)
    for step, copy in enumerate(copies):
        copy.wait_recv()
        total += landed[step].astype(jnp.float32)
    return total


def total_of(own, landed):
    total = own.astype(jnp.float32)
    for step in range(landed.shape[0]):
        total += landed[step].astype(jnp.float32)
    return total


def layer_kernel(
    n_kv, n_tp, features,
    tokens_hbm, lengths_hbm, freq_hbm, gain_hbm, gain_two_hbm, state_hbm,
    wq_hbm, wk_hbm, wv_hbm, wg_hbm, wo_hbm, fg_hbm, fu_hbm, fd_hbm,
    out, state, s, sems,
):
    kv, tp = lax.axis_index("kv"), lax.axis_index("tp")
    chips = n_tp // CORES
    chip, core = tp // CORES, lax.rem(tp, CORES)
    gathered, gathered_two, merged, hidden = s["gathered"], s["gathered_two"], s["merged"], s["hidden"]
    halves, rows = gathered.shape[0], gathered.shape[3]
    batch = n_kv * rows
    names = ("wq", "wk", "wv", "wg", "gain_two", "wo", "fg", "fu", "fd")
    sources = (wq_hbm, wk_hbm, wv_hbm, wg_hbm, gain_two_hbm, wo_hbm, fg_hbm, fu_hbm, fd_hbm)
    pairs = [(tokens_hbm.at[:, h], gathered.at[h, tp]) for h in range(halves)]
    pairs += [(lengths_hbm, s["lengths"]), (freq_hbm, s["freq"]), (gain_hbm, s["gain"])]
    pairs += [(ref, s[name]) for ref, name in zip(sources[:4], names[:4])]
    pairs += [(state_hbm, state)]
    pairs += [(ref, s[name]) for ref, name in zip(sources[4:], names[4:])]
    loads = load_all(pairs, sems["load"])
    order = ["tokens"] * halves + ["lengths", "freq", "gain"] + list(names[:4]) + ["state"] + list(names[4:])

    def ready(*wanted):
        for name, copy in zip(order, loads):
            if name in wanted:
                copy.wait()

    along = [lax.rem(chip + step, chips) * CORES + core for step in range(1, chips)]
    greet([
        ("tp", along + [chip * CORES + 1 - core]),
        ("kv", [lax.rem(kv + step, n_kv) for step in range(1, n_kv)]),
    ])
    open_sends = []

    def pair_of(name, h):
        return sems[name + "_s"].at[h], sems[name + "_r"].at[h]

    def kv_send(name, h, source, target):
        copies = send_all("kv", n_kv, kv, source, target, *pair_of(name, h))
        open_sends.extend(copies)
        return copies

    ready("tokens")
    first_gather = [
        start_gather(gathered.at[h], tp, n_tp, *pair_of("g", h)) for h in range(halves)
    ]
    ready("lengths", "freq", "gain")
    all_rows = halves * rows
    row = lax.broadcasted_iota(jnp.int32, (all_rows, all_rows), 0)
    col = lax.broadcasted_iota(jnp.int32, (all_rows, all_rows), 1)
    spread = jnp.where(row == col, s["lengths"][...].astype(jnp.float32), 0.0)
    angles = jnp.sum(spread, axis=1, keepdims=True) * s["freq"][...]
    cosine, sine = jnp.cos(angles), jnp.sin(angles)
    lane = lax.broadcasted_iota(jnp.int32, angles.shape, 1)
    sine = jnp.where(lane < QK // 2, -sine, sine)

    def normalise(slots, gains):
        x = jnp.concatenate(
            [slots[j].reshape(batch, slots.shape[3]) for j in range(slots.shape[0])], axis=1
        ).astype(jnp.float32)
        squares = jnp.sum(x * x, axis=1, keepdims=True)
        return (x * gains[...]).astype(jnp.bfloat16), square_block(squares).reshape(n_kv, rows, LANES)

    def project(lhs, weight):
        full = jnp.dot(lhs, weight[...], preferred_element_type=jnp.float32)
        return full.astype(jnp.bfloat16).reshape(n_kv, rows, full.shape[1])

    q_width, v_width = s["wq"].shape[1], s["wv"].shape[1]
    units = s["fg"].shape[1]
    heads = q_width // QK
    width = v_width // heads
    out_a, out_b, in_a, in_b = s["out_a"], s["out_b"], s["in_a"], s["in_b"]
    first, second, copies_m = [], [], []

    def project_first(h):
        normed, squares = normalise(gathered.at[h], s["gain"])
        out_a[h, :, :, 2 * q_width :] = squares
        ready_once("wq", "wk", h)
        out_a[h, :, :, :q_width] = project(normed, s["wq"])
        out_a[h, :, :, q_width : 2 * q_width] = project(normed, s["wk"])
        first.append(kv_send("a", h, lambda p: out_a.at[h, p], lambda n: in_a.at[h, n - 1]))
        ready_once("wv", "wg", h)
        out_b[h, :, :, :v_width] = project(normed, s["wv"])
        out_b[h, :, :, v_width:] = project(normed, s["wg"])
        second.append(kv_send("b", h, lambda p: out_b.at[h, p], lambda n: in_b.at[h, n - 1]))

    def ready_once(*args):
        if args[-1] == 0:
            ready(*args[:-1])

    decays = []
    for head in range(heads):
        number = jnp.full((1, width), tp * heads + head, jnp.int32).astype(jnp.float32)
        decays.append(1.0 - jnp.exp2(-5.0 - 10.0 * number / (heads * n_tp - 1)))
    qk, value, retained = s["qk"], s["value"], s["retained"]

    def attend(h):
        base = h * rows
        received(first[h])
        total = total_of(out_a[h, kv], in_a.at[h])
        scale = lax.rsqrt(square_total(total[:, 2 * q_width :]) / features + 1e-06)
        total = total * scale
        cosines, sines = cosine[base : base + rows], sine[base : base + rows]
        blocks = []
        for start, factor in ((0, 1.0), (q_width, QK ** (-0.5))):
            for head in range(heads):
                part = total[:, start + head * QK : start + (head + 1) * QK]
                turned = (part * cosines + pltpu.roll(part, QK // 2, 1) * sines) * factor
                blocks.append(turned.astype(jnp.bfloat16).astype(jnp.float32))
        columns = jnp.concatenate(blocks * (LANES // (len(blocks) * rows)), axis=0).T
        qk[h] = columns
        for i in range(rows):
            for head in range(heads):
                query = columns[:, head * rows + i : head * rows + i + 1]
                retained[base + i : base + i + 1, head * width : (head + 1) * width] = jnp.sum(
                    query * state[base + i, head], axis=0, keepdims=True
                )
        received(second[h])
        total = total_of(out_b[h, kv], in_b.at[h]) * scale
        values = total[:, :v_width].astype(jnp.bfloat16).astype(jnp.float32)
        value[base : base + rows] = values
        pieces = []
        for head in range(heads):
            overlap = jnp.sum(blocks[head] * blocks[heads + head], axis=1, keepdims=True)
            span = slice(head * width, (head + 1) * width)
            piece = decays[head] * retained[base : base + rows, span] + overlap * values[:, span]
            pieces.append(piece * lax.rsqrt(jnp.mean(piece * piece, axis=1, keepdims=True) + 1e-06))
        merged[h, kv] = (jnp.concatenate(pieces, axis=1) * silu(total[:, v_width:])).astype(jnp.bfloat16)
        copies_m.append(kv_send("m", h, lambda p: merged.at[h, kv], lambda n: merged.at[h, kv]))

    block = 8

    def update(h):
        base = h * rows

        def update_step(i, carry):
            start = i * block
            turned = pltpu.roll(qk[h], lax.rem(LANES - start, LANES), 1)
            for n in range(block):
                for head in range(heads):
                    lane = (heads + head) * rows + n
                    at = base + start + n
                    outer = turned[:, lane : lane + 1] * value[pl.ds(at, 1), head * width : (head + 1) * width]
                    state[at, head] = decays[head] * state[at, head] + outer
            return carry

        lax.fori_loop(0, rows // block, update_step, 0)

    def reduce_start(h, lhs, weight, tag):
        return start_reduce(
            lhs, s[weight], s["parts_" + tag].at[h], s["swapped_" + tag].at[h], tp, n_tp, *pair_of(tag, h)
        )

    def reduce_spread(h, swap, tag):
        copies = spread_pairs(
            swap, s["parts_" + tag].at[h], s["swapped_" + tag].at[h], s["staged_" + tag].at[h],
            s["landed_" + tag].at[h], tp, n_tp, *pair_of(tag, h)
        )
        open_sends.extend(copies + [swap])
        return copies

    def reduce_total(h, copies, tag):
        return pairs_total(
            copies, s["parts_" + tag].at[h], s["swapped_" + tag].at[h], s["landed_" + tag].at[h], tp
        )

    gate_out, up_out, gate_in, up_in = s["gate_out"], s["up_out"], s["gate_in"], s["up_in"]
    copies_e, copies_f, copies_h = [], [], []

    def project_second(h):
        normed, squares = normalise(gathered_two.at[h], s["gain_two"])
        gate_out[h, :, :, units:] = squares
        gate_out[h, :, :, :units] = project(normed, s["fg"])
        copies_e.append(kv_send("e", h, lambda p: gate_out.at[h, p], lambda n: gate_in.at[h, n - 1]))
        up_out[h] = project(normed, s["fu"])
        copies_f.append(kv_send("f", h, lambda p: up_out.at[h, p], lambda n: up_in.at[h, n - 1]))

    def activate(h):
        received(copies_e[h])
        total = total_of(gate_out[h, kv], gate_in.at[h])
        scale = lax.rsqrt(square_total(total[:, units:]) / features + 1e-06)
        activated = silu(total[:, :units] * scale)
        received(copies_f[h])
        hidden[h, kv] = (activated * (total_of(up_out[h, kv], up_in.at[h]) * scale)).astype(jnp.bfloat16)
        copies_h.append(kv_send("h", h, lambda p: hidden.at[h, kv], lambda n: hidden.at[h, kv]))

    for relay, _ in first_gather:
        relay()
    for h in range(halves):
        open_sends.extend(first_gather[h][1]())
        project_first(h)
    ready("state")
    for h in range(halves):
        attend(h)
    ready("wo")
    spread_o = []
    for h in range(halves):
        received(copies_m[h])
        swap = reduce_start(h, merged[h].reshape(batch, v_width), "wo", "x")
        spread_o.append(reduce_spread(h, swap, "x"))
        update(h)
    second_gather = []
    for h in range(halves):
        total = reduce_total(h, spread_o[h], "x")
        own = gathered[h, tp].reshape(batch, LANES).astype(jnp.float32)
        gathered_two[h, tp] = (own + total).astype(jnp.bfloat16).reshape(n_kv, rows, LANES)
        second_gather.append(start_gather(gathered_two.at[h], tp, n_tp, *pair_of("c", h)))
    ready("gain_two", "fg", "fu")
    for h in range(halves):
        second_gather[h][0]()
        open_sends.extend(second_gather[h][1]())
        project_second(h)
    for h in range(halves):
        activate(h)
    ready("fd")
    spread_d = []
    for h in range(halves):
        received(copies_h[h])
        swap = reduce_start(h, hidden[h].reshape(batch, units), "fd", "d")
        spread_d.append(reduce_spread(h, swap, "d"))
    for h in range(halves):
        total = reduce_total(h, spread_d[h], "d")
        own = gathered_two[h, tp].reshape(batch, LANES).astype(jnp.float32)
        out[:, h] = (own + total).astype(jnp.bfloat16).reshape(n_kv, rows, LANES)
    sent(open_sends)


def finish_kernel(state, out, state_to, out_to, store_sems):
    chunks = store_sems.shape[0] - 1
    size = state.shape[0] // chunks
    targets = [(out, out_to)]
    for i in range(chunks):
        part = pl.ds(i * size, size)
        targets.append((state.at[part], state_to.at[part]))
    for copy in load_all(targets, store_sems):
        copy.wait()


HALVES = 2


def fused_on_device(n_kv, n_tp, *arrays):
    (
        tokens, lengths, state, mixer_gain, wq, wk, wv, wg, wo, channel_gain, fg, fu, fd,
    ) = arrays
    columns = tokens.shape[1]
    rows = state.shape[0] // HALVES
    batch = n_kv * rows
    depth, q_width = wq.shape
    v_width, units = wv.shape[1], fg.shape[1]
    bf16, f32 = jnp.bfloat16, jnp.float32
    vmem = pl.BlockSpec(memory_space=pltpu.VMEM)
    hbm = pl.BlockSpec(memory_space=pltpu.HBM)
    chips = n_tp // CORES
    index = np.arange(QK) % (QK // 2)
    freq = jnp.asarray((10000.0 ** (-index / (QK // 2))).astype(np.float32))[None, :]
    a_width, b_width = 2 * q_width + LANES, 2 * v_width

    def buffer(*shape, dtype=bf16):
        return pltpu.VMEM((HALVES,) + shape, dtype)

    scratch = {
        "lengths": pltpu.VMEM((1, HALVES * rows), jnp.int32),
        "freq": pltpu.VMEM((1, QK), f32),
        "gain": pltpu.VMEM((1, depth), f32),
        "gain_two": pltpu.VMEM((1, depth), f32),
        "gathered": buffer(n_tp, n_kv, rows, columns),
        "gathered_two": buffer(n_tp, n_kv, rows, columns),
        "out_a": buffer(n_kv, rows, a_width),
        "out_b": buffer(n_kv, rows, b_width),
        "in_a": buffer(n_kv - 1, rows, a_width),
        "in_b": buffer(n_kv - 1, rows, b_width),
        "qk": buffer(QK, LANES, dtype=f32),
        "retained": pltpu.VMEM((HALVES * rows, v_width), f32),
        "value": pltpu.VMEM((HALVES * rows, v_width), f32),
        "merged": buffer(n_kv, rows, v_width),
        "gate_out": buffer(n_kv, rows, units + LANES),
        "up_out": buffer(n_kv, rows, units),
        "gate_in": buffer(n_kv - 1, rows, units + LANES),
        "up_in": buffer(n_kv - 1, rows, units),
        "hidden": buffer(n_kv, rows, units),
    }
    weights = {"wq": wq, "wk": wk, "wv": wv, "wg": wg, "wo": wo, "fg": fg, "fu": fu, "fd": fd}
    scratch.update({name: pltpu.VMEM(w.shape, bf16) for name, w in weights.items()})
    for tag in ("x", "d"):
        scratch["parts_" + tag] = buffer(CORES, chips, batch, columns)
        scratch["swapped_" + tag] = buffer(chips, batch, columns)
        scratch["staged_" + tag] = buffer(chips - 1, batch, columns)
        scratch["landed_" + tag] = buffer(chips - 1, batch, columns)
    counts = {"g": n_tp - 1, "c": n_tp - 1, "x": chips, "d": chips}
    counts.update({tag: n_kv - 1 for tag in ("a", "b", "m", "e", "f", "h")})
    sems = {"load": pltpu.SemaphoreType.DMA((HALVES + 13,))}
    for tag, count in counts.items():
        sems[tag + "_s"] = sems[tag + "_r"] = pltpu.SemaphoreType.DMA((HALVES, count))
    operands = (
        tokens.reshape(n_kv, HALVES, rows, columns), lengths[None, :], freq, mixer_gain[None, :],
        channel_gain[None, :], state, wq, wk, wv, wg, wo, fg, fu, fd,
    )
    out_shape = (n_kv, HALVES, rows, columns)
    out, new_state = pl.pallas_call(
        functools.partial(layer_kernel, n_kv, n_tp, depth * n_kv),
        out_shape=(pltpu.VMEM(out_shape, bf16), pltpu.VMEM(state.shape, f32)),
        in_specs=[hbm] * 14,
        out_specs=(vmem, vmem),
        scratch_shapes=[scratch, sems],
        compiler_params=pltpu.CompilerParams(
            collective_id=0, has_side_effects=True, vmem_limit_bytes=LAYER_VMEM
        ),
        name="layer",
    )(*[pltpu.with_memory_space_constraint(a, pltpu.HBM) for a in operands])
    new_state, out = pl.pallas_call(
        finish_kernel,
        out_shape=(
            jax.ShapeDtypeStruct(state.shape, f32),
            jax.ShapeDtypeStruct(out_shape, bf16),
        ),
        in_specs=[vmem, vmem],
        out_specs=(hbm, hbm),
        scratch_shapes=[pltpu.SemaphoreType.DMA((9,))],
        compiler_params=pltpu.CompilerParams(vmem_limit_bytes=FINISH_VMEM),
        name="finish",
    )(new_state, out)
    return out.reshape(tokens.shape), new_state


def fits(n_kv, n_tp, arrays):
    tokens, state, ffn_gate = arrays[0], arrays[2], arrays[10]
    rows, heads = state.shape[0], state.shape[1]
    return (
        tokens.shape[1] % LANES == 0
        and n_tp % CORES == 0
        and n_tp > CORES
        and n_kv > 1
        and 4 * state.size < VMEM_TOTAL // 4
        and ffn_gate.shape[1] % LANES == 0
        and tokens.shape[1] == LANES
        and tokens.shape[0] == n_kv * rows
        and rows % (16 * HALVES) == 0
        and 2 * heads * rows == LANES
        and state.shape[2] == QK == LANES
        and state.shape[3] % LANES == 0
    )


def per_device(n_kv, n_tp, *arrays):
    if fits(n_kv, n_tp, arrays):
        return fused_on_device(n_kv, n_tp, *arrays)
    return on_device(*arrays)


def solution(mesh):
    in_specs = (
        P(None, ("kv", "tp")),
        P("kv"),
        P("kv", "tp", None, None),
        P("kv"),
        P("kv", "tp"),
        P("kv", "tp"),
        P("kv", "tp"),
        P("kv", "tp"),
        P("tp", "kv"),
        P("kv"),
        P("kv", "tp"),
        P("kv", "tp"),
        P("tp", "kv"),
    )
    out_specs = (P(None, ("kv", "tp")), P("kv", "tp", None, None))
    return jax.shard_map(
        functools.partial(per_device, mesh.shape["kv"], mesh.shape["tp"]),
        mesh=mesh, in_specs=in_specs, out_specs=out_specs, check_vma=False
    )
```

time: 60.9 us -> 54.7 us (0.90)
  Pallas kernels: 60.1 us -> 53.9 us
    pallas_call x1, Pallas kernels: 56.7 us -> 50.5 us  [fused_on_device(): pl.pallas_call(functools.partial(layer_kernel, n_kv, n_tp, depth * n_kv),...]
where the time goes in v2:
time: 54.7 us; the launch traced here: 54.6 us
  Pallas kernels  53.9 us (99%)
  between operations  0.64 us (1%)
    pallas_call x1, Pallas kernels, fused_on_device(): pl.pallas_call(functools.partial(layer_kernel, n_kv, n_tp, depth * n_kv),...  50.5 us
    pallas_call x1, Pallas kernels, fused_on_device(): pl.pallas_call(finish_kernel, out_shape=(jax.ShapeDtypeStruct(state.shape...  3.39 us

profile of v2, /device:TPU:0, one launch (start us, length us, event | category | flops | bytes accessed | tf_op | source)
XLA Modules:
  0.0 54.6 jit_solution(14037245840794289004)
XLA Ops:
  0.6 50.5 %layer.1 = (bf16[4,2,16,128]{3,2,1,0:T(8,128)(2,1)S(1)}, f32[32,2,128,256]{3,2,1,0:T(8,128)S(1)}) custom-call(bf16[4,2,16,128]{3,2,1,0:T(8,128)(2,1)} %bitcast.5, s32[1,32]{1,0:T(1,128)} %bitcast.8, f32[1,128]{1,0:T(1,128)} %constant.4.freq_hbm, f32[1,1024]{1,0:T(1,128)} %bitcast.6, f32[1,1024]{1,0:T(1,128)} %bitcast.7, f32[32,2,128,256]{3,2,1,0:T(8,128)} %state_hbm.1, ...), custom_call_target="tpu_custom_call" | custom-call | tf_op jit(solution)/shard_map/layer/pallas_call | solution.py:603
  51.2 3.4 %finish.1 = (f32[32,2,128,256]{3,2,1,0:T(8,128)}, bf16[4,2,16,128]{3,2,1,0:T(8,128)(2,1)}) custom-call(f32[32,2,128,256]{3,2,1,0:T(8,128)S(1)} %get-tuple-element.6.state, bf16[4,2,16,128]{3,2,1,0:T(8,128)(2,1)S(1)} %get-tuple-element.7.out), custom_call_target="tpu_custom_call" | custom-call | tf_op jit(solution)/shard_map/finish/pallas_call | solution.py:614

commit v3 on v2

--- a/solution.py
+++ b/solution.py
@@ -146,158 +146,144 @@
 MESH_ID = pl.DeviceIdType.MESH
 VMEM_TOTAL = 67043328
 CORES = 2
+SIDE = 2
 LAYER_VMEM = 50000000
 FINISH_VMEM = 20000000
 
 
-def greet(groups):
+def greet(devices):
     barrier = pltpu.get_barrier_semaphore()
-    for axis, peers in groups:
-        for peer in peers:
-            pl.semaphore_signal(barrier, inc=1, device_id={axis: peer}, device_id_type=MESH_ID)
-    pl.semaphore_wait(barrier, sum(len(peers) for _, peers in groups))
-
-
-def send_all(axis, count, me, source, target, send_sems, recv_sems):
-    copies = []
-    for step in range(1, count):
-        peer = lax.rem(me + step, count)
-        copy = pltpu.make_async_remote_copy(
-            src_ref=source(peer),
-            dst_ref=target(step),
-            send_sem=send_sems.at[step - 1],
-            recv_sem=recv_sems.at[step - 1],
-            device_id={axis: peer},
-            device_id_type=MESH_ID,
-        )
-        copy.start()
-        copies.append(copy)
-    return copies
-
-
-def received(copies):
-    for copy in copies:
-        copy.wait_recv()
-
-
-def sent(copies):
-    for copy in copies:
-        copy.wait_send()
-
-
-def load_all(pairs, sems):
-    copies = [pltpu.make_async_copy(src, dst, sems.at[i]) for i, (src, dst) in enumerate(pairs)]
-    for copy in copies:
-        copy.start()
-    return copies
+    for device in devices:
+        pl.semaphore_signal(barrier, inc=1, device_id=device, device_id_type=MESH_ID)
+    pl.semaphore_wait(barrier, len(devices))
+
+
+def kv_peers(kv, n_kv):
+    return [n_kv - 1 - kv, kv + 1 - 2 * lax.rem(kv, SIDE), lax.rem(kv + SIDE, n_kv)]
+
+
+def send_all(devices, source, target, send_sem, recv_sem):
+    for k, device in enumerate(devices):
+        remote_to(device, source(device["kv"]), target(k), send_sem, recv_sem).start()
+
+
+def landed(ref, sem):
+    pltpu.make_async_copy(ref, ref, sem).wait()
+
+
+def load_all(pairs, sem):
+    for source, target in pairs:
+        pltpu.make_async_copy(source, target, sem).start()
 
 
 def silu(value):
     return value / (1.0 + jnp.exp(-value))
 
 
-def square_block(squares):
-    head = squares.astype(jnp.bfloat16).astype(jnp.float32)
-    rest = squares - head
-    lane = lax.broadcasted_iota(jnp.int32, (squares.shape[0], LANES), 1)
-    return jnp.where(lane < LANES // 2, head, rest).astype(jnp.bfloat16)
-
-
-def square_total(block):
-    return block[:, :1] + block[:, LANES // 2 : LANES // 2 + 1]
+def as_row(column):
+    lane = lax.broadcasted_iota(jnp.int32, (column.shape[0], LANES), 1)
+    row = lax.broadcasted_iota(jnp.int32, (column.shape[0], LANES), 0)
+    return jnp.sum(jnp.where(row == lane, column, 0.0), axis=0, keepdims=True)
+
+
+def as_column(row_values, first, rows):
+    lane = lax.broadcasted_iota(jnp.int32, (rows, LANES), 1)
+    row = lax.broadcasted_iota(jnp.int32, (rows, LANES), 0)
+    return jnp.sum(jnp.where(row + first == lane, row_values, 0.0), axis=1, keepdims=True)
 
 
 def remote(axis, peer, source, target, send_sem, recv_sem):
+    return remote_to({axis: peer}, source, target, send_sem, recv_sem)
+
+
+def remote_to(device, source, target, send_sem, recv_sem):
     return pltpu.make_async_remote_copy(
         src_ref=source, dst_ref=target, send_sem=send_sem, recv_sem=recv_sem,
-        device_id={axis: peer}, device_id_type=MESH_ID,
-    )
-
-
-def start_gather(slots, tp, n_tp, send_sems, recv_sems):
+        device_id=device, device_id_type=MESH_ID,
+    )
+
+
+def far_first(chip, chips):
+    def ascending(at, k):
+        return k + 1 - (at + chips - 1 - k) // chips
+
+    low = 1 - chip // (chips // 2)
+    mirrored = chips - 1 - chip
+    return [
+        low * (chips - 1 - ascending(mirrored, k)) + (1 - low) * ascending(chip, k)
+        for k in range(chips - 1)
+    ]
+
+
+def start_gather(slots, tp, n_tp, hub, send_sems, recv_sems):
     chips = n_tp // CORES
     chip, core = tp // CORES, lax.rem(tp, CORES)
     partner = chip * CORES + 1 - core
-    direct = []
-    for step in range(1, chips):
-        peer = lax.rem(chip + step, chips) * CORES + core
-        direct.append(
-            remote("tp", peer, slots.at[tp], slots.at[tp], send_sems.at[step], recv_sems.at[step])
-        )
-    across = [remote("tp", partner, slots.at[tp], slots.at[tp], send_sems.at[0], recv_sems.at[0])]
-    for copy in direct + across:
-        copy.start()
-
-    def relay():
-        for step in range(1, chips):
-            direct[step - 1].wait_recv()
-            slot = lax.rem(chip - step + chips, chips) * CORES + core
-            i = chips - 1 + step
-            copy = remote(
-                "tp", partner, slots.at[slot], slots.at[slot], send_sems.at[i], recv_sems.at[i]
-            )
-            copy.start()
-            across.append(copy)
-
-    def finish():
-        received(across)
-        return direct + across
-
-    return relay, finish
-
-
-def start_reduce(lhs, weight, parts, swapped, tp, n_tp, send_sems, recv_sems):
-    chips = n_tp // CORES
+    order = far_first(chip, chips)
+
+    def block(peer, slot, send):
+        return remote("tp", peer, slots.at[slot], slots.at[slot], send_sems.at[send], recv_sems.at[slot])
+
+    for peer in order:
+        block(peer * CORES + hub, tp, 0).start()
+    block(partner, tp, 0).start()
+    relayed = [
+        block(partner, source * CORES + side, 1) for source in order[::-1] for side in range(CORES)
+    ]
+
+    def take(first, last):
+        for copy in relayed[first * CORES : last * CORES]:
+            copy.wait_recv()
+
+            @pl.when(core == hub)
+            def _():
+                copy.start()
+
+    def take_own():
+        block(partner, partner, 0).wait_recv()
+
+    def close():
+        landed(slots.at[:chips], send_sems.at[0])
+
+        @pl.when(core == hub)
+        def _():
+            landed(slots.at[: len(relayed)], send_sems.at[1])
+
+    return take, take_own, close
+
+
+def start_reduce(lhs, weight, parts, swapped, tp, send_sems, recv_sems):
     chip, core = tp // CORES, lax.rem(tp, CORES)
-    columns = parts.shape[3]
+    chips, columns = parts.shape[1], parts.shape[3]
 
     def multiply(side):
-        starts = [pl.multiple_of((z * CORES + side) * columns, LANES) for z in range(chips)]
-        rhs = jnp.concatenate([weight[:, pl.ds(start, columns)] for start in starts], axis=1)
-        full = jnp.dot(lhs, rhs, preferred_element_type=jnp.float32).astype(jnp.bfloat16)
+        full = jnp.dot(lhs, weight[side], preferred_element_type=jnp.float32).astype(jnp.bfloat16)
         for z in range(chips):
             parts[side, z] = full[:, z * columns : (z + 1) * columns]
 
+    multiply(core)
+    remote(
+        "tp", chip * CORES + 1 - core, parts.at[core], swapped, send_sems.at[0], recv_sems.at[0]
+    ).start()
     multiply(1 - core)
-    swap = remote(
-        "tp", chip * CORES + 1 - core, parts.at[1 - core], swapped, send_sems.at[0], recv_sems.at[0]
-    )
-    swap.start()
-    multiply(core)
-    return swap
-
-
-def spread_pairs(swap, parts, swapped, staged, landed, tp, n_tp, send_sems, recv_sems):
-    chips = n_tp // CORES
+
+
+def spread_pairs(parts, swapped, staged, into, tp, send_sems, recv_sems):
+    chips = parts.shape[1]
     chip, core = tp // CORES, lax.rem(tp, CORES)
-    swap.wait_recv()
-    copies = []
-    for step in range(1, chips):
-        other = lax.rem(chip + step, chips)
-        pair = parts[core, other].astype(jnp.float32) + swapped[other].astype(jnp.float32)
-        staged[step - 1] = pair.astype(jnp.bfloat16)
-        copy = remote(
-            "tp", other * CORES + core, staged.at[step - 1], landed.at[step - 1],
-            send_sems.at[step], recv_sems.at[step],
-        )
-        copy.start()
-        copies.append(copy)
-    return copies
-
-
-def pairs_total(copies, parts, swapped, landed, tp):
-    chip, core = tp // CORES, lax.rem(tp, CORES)
-    total = parts[core, chip].astype(jnp.float32) + swapped[chip].astype(jnp.float32)
-    for step, copy in enumerate(copies):
-        copy.wait_recv()
-        total += landed[step].astype(jnp.float32)
-    return total
-
-
-def total_of(own, landed):
+    landed(swapped, recv_sems.at[0])
+    for k, other in enumerate(far_first(chip, chips) + [chip]):
+        pair = parts[1 - core, other].astype(jnp.float32) + swapped[other].astype(jnp.float32)
+        staged[k] = pair.astype(jnp.bfloat16)
+        remote(
+            "tp", other * CORES + 1 - core, staged.at[k], into.at[chip], send_sems.at[1], recv_sems.at[1]
+        ).start()
+
+
+def total_of(own, others):
     total = own.astype(jnp.float32)
-    for step in range(landed.shape[0]):
-        total += landed[step].astype(jnp.float32)
+    for step in range(others.shape[0]):
+        total += others[step].astype(jnp.float32)
     return total
 
 
@@ -313,40 +299,81 @@
     gathered, gathered_two, merged, hidden = s["gathered"], s["gathered_two"], s["merged"], s["hidden"]
     halves, rows = gathered.shape[0], gathered.shape[3]
     batch = n_kv * rows
-    names = ("wq", "wk", "wv", "wg", "gain_two", "wo", "fg", "fu", "fd")
-    sources = (wq_hbm, wk_hbm, wv_hbm, wg_hbm, gain_two_hbm, wo_hbm, fg_hbm, fu_hbm, fd_hbm)
-    pairs = [(tokens_hbm.at[:, h], gathered.at[h, tp]) for h in range(halves)]
-    pairs += [(lengths_hbm, s["lengths"]), (freq_hbm, s["freq"]), (gain_hbm, s["gain"])]
-    pairs += [(ref, s[name]) for ref, name in zip(sources[:4], names[:4])]
-    pairs += [(state_hbm, state)]
-    pairs += [(ref, s[name]) for ref, name in zip(sources[4:], names[4:])]
-    loads = load_all(pairs, sems["load"])
-    order = ["tokens"] * halves + ["lengths", "freq", "gain"] + list(names[:4]) + ["state"] + list(names[4:])
+    q_width, v_width = wq_hbm.shape[1], wv_hbm.shape[1]
+    units, columns = fg_hbm.shape[1], tokens_hbm.shape[3]
+
+    def sides(ref, target):
+        return [
+            (
+                ref.at[:, (z * CORES + side) * columns : (z * CORES + side + 1) * columns],
+                target.at[side, :, z * columns : (z + 1) * columns],
+            )
+            for side in range(CORES)
+            for z in range(chips)
+        ]
+
+    groups = {
+        "tokens": [(tokens_hbm.at[:, h], gathered.at[h, tp]) for h in range(halves)],
+        "lengths": [(lengths_hbm, s["lengths"])],
+        "freq": [(freq_hbm, s["freq"])],
+        "gain": [(gain_hbm, s["gain"])],
+        "wqk": [(wq_hbm, s["wqk"].at[:, :q_width]), (wk_hbm, s["wqk"].at[:, q_width:])],
+        "wvg": [(wv_hbm, s["wvg"].at[:, :v_width]), (wg_hbm, s["wvg"].at[:, v_width:])],
+        "state": [(state_hbm, state)],
+        "wo": sides(wo_hbm, s["wo"]),
+        "gain_two": [(gain_two_hbm, s["gain_two"])],
+        "fg": [(fg_hbm, s["fg"])],
+        "fu": [(fu_hbm, s["fu"])],
+        "fd": sides(fd_hbm, s["fd"]),
+    }
+    wholes = {
+        "tokens": gathered.at[:, tp], "wqk": s["wqk"], "wvg": s["wvg"], "state": state, "wo": s["wo"], "fd": s["fd"],
+        "lengths": s["lengths"], "freq": s["freq"], "gain": s["gain"],
+        "gain_two": s["gain_two"], "fg": s["fg"], "fu": s["fu"],
+    }
+    pending = {}
+    for i, (name, group) in enumerate(groups.items()):
+        pending[name] = i
+        load_all(group, sems["load"].at[i])
 
     def ready(*wanted):
-        for name, copy in zip(order, loads):
-            if name in wanted:
-                copy.wait()
-
-    along = [lax.rem(chip + step, chips) * CORES + core for step in range(1, chips)]
-    greet([
-        ("tp", along + [chip * CORES + 1 - core]),
-        ("kv", [lax.rem(kv + step, n_kv) for step in range(1, n_kv)]),
-    ])
-    open_sends = []
+        for name in wanted:
+            if name in pending:
+                landed(wholes[name], sems["load"].at[pending.pop(name)])
+
+    partner = chip * CORES + 1 - core
+    peers = [{"kv": peer, "tp": tp} for peer in kv_peers(kv, n_kv)]
+    crossed = [{"kv": peer, "tp": partner} for peer in kv_peers(kv, n_kv)]
+    along = [{"kv": kv, "tp": other * CORES + 1 - core} for other in far_first(chip, chips)]
+    beside = {"kv": kv, "tp": partner}
+    aside = [{"kv": kv, "tp": other * CORES + core} for other in far_first(chip, chips)]
+    greet(along + aside + [beside] + peers + crossed)
+    closing = []
 
     def pair_of(name, h):
         return sems[name + "_s"].at[h], sems[name + "_r"].at[h]
 
-    def kv_send(name, h, source, target):
-        copies = send_all("kv", n_kv, kv, source, target, *pair_of(name, h))
-        open_sends.extend(copies)
-        return copies
+    def kv_send(name, h, devices, source, target, extent):
+        send_sem, recv_sem = sems[name].at[h, 0], sems[name].at[h, 1]
+        send_all(devices, source, target, send_sem, recv_sem)
+        closing.append((extent, send_sem))
+        return lambda: landed(extent, recv_sem)
+
+    def send_squares(name, h, squares):
+        s[name][h, n_kv - 1] = squares
+        return kv_send(
+            name, h, crossed, lambda p: s[name].at[h, n_kv - 1], lambda n: s[name].at[h, n], s[name].at[h, : n_kv - 1]
+        )
+
+    def scale_of(name, h, wait):
+        wait()
+        total = s[name][h, 0]
+        for n in range(1, n_kv):
+            total += s[name][h, n]
+        return lax.rsqrt(as_column(total, kv * rows, rows) / features + 1e-06)
 
     ready("tokens")
-    first_gather = [
-        start_gather(gathered.at[h], tp, n_tp, *pair_of("g", h)) for h in range(halves)
-    ]
+    first_gather = [start_gather(gathered.at[0], tp, n_tp, 0, *pair_of("g", 0))]
     ready("lengths", "freq", "gain")
     all_rows = halves * rows
     row = lax.broadcasted_iota(jnp.int32, (all_rows, all_rows), 0)
@@ -362,34 +389,26 @@
             [slots[j].reshape(batch, slots.shape[3]) for j in range(slots.shape[0])], axis=1
         ).astype(jnp.float32)
         squares = jnp.sum(x * x, axis=1, keepdims=True)
-        return (x * gains[...]).astype(jnp.bfloat16), square_block(squares).reshape(n_kv, rows, LANES)
+        return (x * gains[...]).astype(jnp.bfloat16), as_row(squares)
 
     def project(lhs, weight):
         full = jnp.dot(lhs, weight[...], preferred_element_type=jnp.float32)
         return full.astype(jnp.bfloat16).reshape(n_kv, rows, full.shape[1])
 
-    q_width, v_width = s["wq"].shape[1], s["wv"].shape[1]
-    units = s["fg"].shape[1]
     heads = q_width // QK
     width = v_width // heads
     out_a, out_b, in_a, in_b = s["out_a"], s["out_b"], s["in_a"], s["in_b"]
-    first, second, copies_m = [], [], []
+    first, second, copies_m, copies_q = [], [], [], []
 
     def project_first(h):
         normed, squares = normalise(gathered.at[h], s["gain"])
-        out_a[h, :, :, 2 * q_width :] = squares
-        ready_once("wq", "wk", h)
-        out_a[h, :, :, :q_width] = project(normed, s["wq"])
-        out_a[h, :, :, q_width : 2 * q_width] = project(normed, s["wk"])
-        first.append(kv_send("a", h, lambda p: out_a.at[h, p], lambda n: in_a.at[h, n - 1]))
-        ready_once("wv", "wg", h)
-        out_b[h, :, :, :v_width] = project(normed, s["wv"])
-        out_b[h, :, :, v_width:] = project(normed, s["wg"])
-        second.append(kv_send("b", h, lambda p: out_b.at[h, p], lambda n: in_b.at[h, n - 1]))
-
-    def ready_once(*args):
-        if args[-1] == 0:
-            ready(*args[:-1])
+        ready("wqk")
+        out_a[h] = project(normed, s["wqk"])
+        first.append(kv_send("a", h, peers, lambda p: out_a.at[h, p], lambda n: in_a.at[h, n], in_a.at[h]))
+        ready("wvg")
+        out_b[h] = project(normed, s["wvg"])
+        copies_q.append(send_squares("squares", h, squares))
+        second.append(kv_send("b", h, peers, lambda p: out_b.at[h, p], lambda n: in_b.at[h, n], in_b.at[h]))
 
     decays = []
     for head in range(heads):
@@ -399,9 +418,9 @@
 
     def attend(h):
         base = h * rows
-        received(first[h])
+        first[h]()
         total = total_of(out_a[h, kv], in_a.at[h])
-        scale = lax.rsqrt(square_total(total[:, 2 * q_width :]) / features + 1e-06)
+        scale = scale_of("squares", h, copies_q[h])
         total = total * scale
         cosines, sines = cosine[base : base + rows], sine[base : base + rows]
         blocks = []
@@ -418,7 +437,7 @@
                 retained[base + i : base + i + 1, head * width : (head + 1) * width] = jnp.sum(
                     query * state[base + i, head], axis=0, keepdims=True
                 )
-        received(second[h])
+        second[h]()
         total = total_of(out_b[h, kv], in_b.at[h]) * scale
         values = total[:, :v_width].astype(jnp.bfloat16).astype(jnp.float32)
         value[base : base + rows] = values
@@ -429,7 +448,9 @@
             piece = decays[head] * retained[base : base + rows, span] + overlap * values[:, span]
             pieces.append(piece * lax.rsqrt(jnp.mean(piece * piece, axis=1, keepdims=True) + 1e-06))
         merged[h, kv] = (jnp.concatenate(pieces, axis=1) * silu(total[:, v_width:])).astype(jnp.bfloat16)
-        copies_m.append(kv_send("m", h, lambda p: merged.at[h, kv], lambda n: merged.at[h, kv]))
+        copies_m.append(kv_send(
+            "m", h, peers, lambda p: merged.at[h, kv], lambda n: merged.at[h, kv], merged.at[h, : n_kv - 1]
+        ))
 
     block = 8
 
@@ -450,82 +471,91 @@
         lax.fori_loop(0, rows // block, update_step, 0)
 
     def reduce_start(h, lhs, weight, tag):
-        return start_reduce(
-            lhs, s[weight], s["parts_" + tag].at[h], s["swapped_" + tag].at[h], tp, n_tp, *pair_of(tag, h)
-        )
-
-    def reduce_spread(h, swap, tag):
-        copies = spread_pairs(
-            swap, s["parts_" + tag].at[h], s["swapped_" + tag].at[h], s["staged_" + tag].at[h],
-            s["landed_" + tag].at[h], tp, n_tp, *pair_of(tag, h)
-        )
-        open_sends.extend(copies + [swap])
-        return copies
-
-    def reduce_total(h, copies, tag):
-        return pairs_total(
-            copies, s["parts_" + tag].at[h], s["swapped_" + tag].at[h], s["landed_" + tag].at[h], tp
-        )
+        start_reduce(lhs, s[weight], s["parts_" + tag].at[h], s["swapped_" + tag].at[h], tp, *pair_of(tag, h))
+
+    def reduce_spread(h, tag):
+        swapped, staged = s["swapped_" + tag].at[h], s["staged_" + tag].at[h]
+        send_sems, recv_sems = pair_of(tag, h)
+        spread_pairs(s["parts_" + tag].at[h], swapped, staged, s["landed_" + tag].at[h], tp, send_sems, recv_sems)
+        closing.extend([(swapped, send_sems.at[0]), (staged, send_sems.at[1])])
+
+    def reduce_total(h, tag):
+        into = s["landed_" + tag].at[h]
+        landed(into, pair_of(tag, h)[1].at[1])
+        return total_of(into[0], into.at[1:])
 
     gate_out, up_out, gate_in, up_in = s["gate_out"], s["up_out"], s["gate_in"], s["up_in"]
-    copies_e, copies_f, copies_h = [], [], []
+    copies_e, copies_f, copies_h, copies_u = [], [], [], []
+    crossed_all = crossed + [beside]
 
     def project_second(h):
         normed, squares = normalise(gathered_two.at[h], s["gain_two"])
-        gate_out[h, :, :, units:] = squares
-        gate_out[h, :, :, :units] = project(normed, s["fg"])
-        copies_e.append(kv_send("e", h, lambda p: gate_out.at[h, p], lambda n: gate_in.at[h, n - 1]))
+        gate_out[h] = project(normed, s["fg"])
+        copies_e.append(
+            kv_send("e", h, crossed_all, lambda p: gate_out.at[h, p], lambda n: gate_in.at[h, n], gate_in.at[h])
+        )
+        copies_u.append(send_squares("squares_two", h, squares))
         up_out[h] = project(normed, s["fu"])
-        copies_f.append(kv_send("f", h, lambda p: up_out.at[h, p], lambda n: up_in.at[h, n - 1]))
+        copies_f.append(
+            kv_send("f", h, crossed_all, lambda p: up_out.at[h, p], lambda n: up_in.at[h, n], up_in.at[h])
+        )
 
     def activate(h):
-        received(copies_e[h])
-        total = total_of(gate_out[h, kv], gate_in.at[h])
-        scale = lax.rsqrt(square_total(total[:, units:]) / features + 1e-06)
-        activated = silu(total[:, :units] * scale)
-        received(copies_f[h])
-        hidden[h, kv] = (activated * (total_of(up_out[h, kv], up_in.at[h]) * scale)).astype(jnp.bfloat16)
-        copies_h.append(kv_send("h", h, lambda p: hidden.at[h, kv], lambda n: hidden.at[h, kv]))
-
-    for relay, _ in first_gather:
-        relay()
+        copies_e[h]()
+        total = total_of(gate_in[h, 0], gate_in.at[h, 1:])
+        scale = scale_of("squares_two", h, copies_u[h])
+        activated = silu(total * scale)
+        copies_f[h]()
+        up = total_of(up_in[h, 0], up_in.at[h, 1:]) * scale
+        s["hidden_out"][h] = (activated * up).astype(jnp.bfloat16)
+        copies_h.append(
+            kv_send("h", h, crossed_all, lambda p: s["hidden_out"].at[h], lambda n: hidden.at[h, kv], hidden.at[h])
+        )
+
+    first_gather[0][0](0, 1)
+    for h in range(1, halves):
+        first_gather.append(start_gather(gathered.at[h], tp, n_tp, 0, *pair_of("g", h)))
+    first_gather[0][0](1, chips - 1)
     for h in range(halves):
-        open_sends.extend(first_gather[h][1]())
+        if h > 0:
+            first_gather[h][0](0, chips - 1)
+        first_gather[h][1]()
         project_first(h)
     ready("state")
     for h in range(halves):
         attend(h)
     ready("wo")
-    spread_o = []
     for h in range(halves):
-        received(copies_m[h])
-        swap = reduce_start(h, merged[h].reshape(batch, v_width), "wo", "x")
-        spread_o.append(reduce_spread(h, swap, "x"))
+        copies_m[h]()
+        reduce_start(h, merged[h].reshape(batch, v_width), "wo", "x")
+        reduce_spread(h, "x")
         update(h)
     second_gather = []
     for h in range(halves):
-        total = reduce_total(h, spread_o[h], "x")
+        total = reduce_total(h, "x")
         own = gathered[h, tp].reshape(batch, LANES).astype(jnp.float32)
         gathered_two[h, tp] = (own + total).astype(jnp.bfloat16).reshape(n_kv, rows, LANES)
-        second_gather.append(start_gather(gathered_two.at[h], tp, n_tp, *pair_of("c", h)))
+        second_gather.append(start_gather(gathered_two.at[h], tp, n_tp, 1, *pair_of("c", h)))
     ready("gain_two", "fg", "fu")
     for h in range(halves):
-        second_gather[h][0]()
-        open_sends.extend(second_gather[h][1]())
+        second_gather[h][1]()
+        second_gather[h][0](0, chips - 1)
         project_second(h)
     for h in range(halves):
         activate(h)
     ready("fd")
-    spread_d = []
     for h in range(halves):
-        received(copies_h[h])
-        swap = reduce_start(h, hidden[h].reshape(batch, units), "fd", "d")
-        spread_d.append(reduce_spread(h, swap, "d"))
+        copies_h[h]()
+        reduce_start(h, hidden[h].reshape(batch, units), "fd", "d")
+        reduce_spread(h, "d")
     for h in range(halves):
-        total = reduce_total(h, spread_d[h], "d")
+        total = reduce_total(h, "d")
         own = gathered_two[h, tp].reshape(batch, LANES).astype(jnp.float32)
         out[:, h] = (own + total).astype(jnp.bfloat16).reshape(n_kv, rows, LANES)
-    sent(open_sends)
+    for extent, sem in closing:
+        landed(extent, sem)
+    for gather in first_gather + second_gather:
+        gather[2]()
 
 
 def finish_kernel(state, out, state_to, out_to, store_sems):
@@ -535,7 +565,12 @@
     for i in range(chunks):
         part = pl.ds(i * size, size)
         targets.append((state.at[part], state_to.at[part]))
-    for copy in load_all(targets, store_sems):
+    copies = [
+        pltpu.make_async_copy(source, target, store_sems.at[i]) for i, (source, target) in enumerate(targets)
+    ]
+    for copy in copies:
+        copy.start()
+    for copy in copies:
         copy.wait()
 
 
@@ -557,7 +592,7 @@
     chips = n_tp // CORES
     index = np.arange(QK) % (QK // 2)
     freq = jnp.asarray((10000.0 ** (-index / (QK // 2))).astype(np.float32))[None, :]
-    a_width, b_width = 2 * q_width + LANES, 2 * v_width
+    a_width, b_width = 2 * q_width, 2 * v_width
 
     def buffer(*shape, dtype=bf16):
         return pltpu.VMEM((HALVES,) + shape, dtype)
@@ -577,24 +612,33 @@
         "retained": pltpu.VMEM((HALVES * rows, v_width), f32),
         "value": pltpu.VMEM((HALVES * rows, v_width), f32),
         "merged": buffer(n_kv, rows, v_width),
-        "gate_out": buffer(n_kv, rows, units + LANES),
+        "gate_out": buffer(n_kv, rows, units),
         "up_out": buffer(n_kv, rows, units),
-        "gate_in": buffer(n_kv - 1, rows, units + LANES),
-        "up_in": buffer(n_kv - 1, rows, units),
+        "gate_in": buffer(n_kv, rows, units),
+        "up_in": buffer(n_kv, rows, units),
+        "hidden_out": buffer(rows, units),
         "hidden": buffer(n_kv, rows, units),
+        "squares": buffer(n_kv, 1, LANES, dtype=f32),
+        "squares_two": buffer(n_kv, 1, LANES, dtype=f32),
     }
-    weights = {"wq": wq, "wk": wk, "wv": wv, "wg": wg, "wo": wo, "fg": fg, "fu": fu, "fd": fd}
-    scratch.update({name: pltpu.VMEM(w.shape, bf16) for name, w in weights.items()})
+    shapes = {
+        "wqk": (depth, 2 * q_width), "wvg": (depth, 2 * v_width), "fg": fg.shape, "fu": fu.shape,
+        "wo": (CORES, wo.shape[0], chips * columns), "fd": (CORES, fd.shape[0], chips * columns),
+    }
+    scratch.update({name: pltpu.VMEM(shape, bf16) for name, shape in shapes.items()})
     for tag in ("x", "d"):
         scratch["parts_" + tag] = buffer(CORES, chips, batch, columns)
         scratch["swapped_" + tag] = buffer(chips, batch, columns)
-        scratch["staged_" + tag] = buffer(chips - 1, batch, columns)
-        scratch["landed_" + tag] = buffer(chips - 1, batch, columns)
-    counts = {"g": n_tp - 1, "c": n_tp - 1, "x": chips, "d": chips}
-    counts.update({tag: n_kv - 1 for tag in ("a", "b", "m", "e", "f", "h")})
-    sems = {"load": pltpu.SemaphoreType.DMA((HALVES + 13,))}
-    for tag, count in counts.items():
-        sems[tag + "_s"] = sems[tag + "_r"] = pltpu.SemaphoreType.DMA((HALVES, count))
+        scratch["staged_" + tag] = buffer(chips, batch, columns)
+        scratch["landed_" + tag] = buffer(chips, batch, columns)
+    dma = pltpu.SemaphoreType.DMA
+    sems = {"load": dma((12,))}
+    for tag in ("g", "c"):
+        sems[tag + "_s"], sems[tag + "_r"] = dma((HALVES, 2)), dma((HALVES, n_tp))
+    for tag in ("x", "d"):
+        sems[tag + "_s"] = sems[tag + "_r"] = dma((HALVES, 2))
+    for tag in ("a", "b", "m", "e", "f", "h", "squares", "squares_two"):
+        sems[tag] = dma((HALVES, 2))
     operands = (
         tokens.reshape(n_kv, HALVES, rows, columns), lengths[None, :], freq, mixer_gain[None, :],
         channel_gain[None, :], state, wq, wk, wv, wg, wo, fg, fu, fd,
@@ -633,12 +677,13 @@
         tokens.shape[1] % LANES == 0
         and n_tp % CORES == 0
         and n_tp > CORES
-        and n_kv > 1
+        and n_kv == SIDE * SIDE
         and 4 * state.size < VMEM_TOTAL // 4
         and ffn_gate.shape[1] % LANES == 0
         and tokens.shape[1] == LANES
         and tokens.shape[0] == n_kv * rows
         and rows % (16 * HALVES) == 0
+        and n_kv * rows // HALVES <= LANES
         and 2 * heads * rows == LANES
         and state.shape[2] == QK == LANES
         and state.shape[3] % LANES == 0

time: 54.7 us -> 51.7 us (0.945)
  Pallas kernels: 53.9 us -> 50.9 us
    pallas_call x1, Pallas kernels: 50.5 us -> 47.5 us  [fused_on_device(): pl.pallas_call(functools.partial(layer_kernel, n_kv, n_tp, depth * n_kv),...]
where the time goes in v3:
time: 51.7 us; the launch traced here: 51.5 us
  Pallas kernels  50.9 us (98%)
  between operations  0.64 us (1%)
    pallas_call x1, Pallas kernels, fused_on_device(): pl.pallas_call(functools.partial(layer_kernel, n_kv, n_tp, depth * n_kv),...  47.5 us
    pallas_call x1, Pallas kernels, fused_on_device(): pl.pallas_call(finish_kernel, out_shape=(jax.ShapeDtypeStruct(state.shape...  3.39 us

profile of v3, /device:TPU:0, one launch (start us, length us, event | category | flops | bytes accessed | tf_op | source)
XLA Modules:
  0.0 51.5 jit_solution(848028551539511744)
XLA Ops:
  0.6 47.5 %layer.1 = (bf16[4,2,16,128]{3,2,1,0:T(8,128)(2,1)S(1)}, f32[32,2,128,256]{3,2,1,0:T(8,128)S(1)}) custom-call(bf16[4,2,16,128]{3,2,1,0:T(8,128)(2,1)} %bitcast.5, s32[1,32]{1,0:T(1,128)} %bitcast.8, f32[1,128]{1,0:T(1,128)} %constant.4.freq_hbm, f32[1,1024]{1,0:T(1,128)} %bitcast.6, f32[1,1024]{1,0:T(1,128)} %bitcast.7, f32[32,2,128,256]{3,2,1,0:T(8,128)} %state_hbm.1, ...), custom_call_target="tpu_custom_call" | custom-call | tf_op jit(solution)/shard_map/layer/pallas_call | solution.py:647
  48.1 3.4 %finish.1 = (f32[32,2,128,256]{3,2,1,0:T(8,128)}, bf16[4,2,16,128]{3,2,1,0:T(8,128)(2,1)}) custom-call(f32[32,2,128,256]{3,2,1,0:T(8,128)S(1)} %get-tuple-element.6.state, bf16[4,2,16,128]{3,2,1,0:T(8,128)(2,1)S(1)} %get-tuple-element.7.out), custom_call_target="tpu_custom_call" | custom-call | tf_op jit(solution)/shard_map/finish/pallas_call | solution.py:658

commit v4 on v3

--- a/solution.py
+++ b/solution.py
@@ -350,19 +350,23 @@
     greet(along + aside + [beside] + peers + crossed)
     closing = []
 
+    def close_sends():
+        for extent, sem in closing:
+            landed(extent, sem)
+        closing.clear()
+
     def pair_of(name, h):
         return sems[name + "_s"].at[h], sems[name + "_r"].at[h]
 
     def kv_send(name, h, devices, source, target, extent):
-        send_sem, recv_sem = sems[name].at[h, 0], sems[name].at[h, 1]
+        send_sem, recv_sem = sems[SHARED.get(name, name)].at[h, 0], sems[SHARED.get(name, name)].at[h, 1]
         send_all(devices, source, target, send_sem, recv_sem)
         closing.append((extent, send_sem))
         return lambda: landed(extent, recv_sem)
 
-    def send_squares(name, h, squares):
-        s[name][h, n_kv - 1] = squares
+    def send_squares(name, h, devices):
         return kv_send(
-            name, h, crossed, lambda p: s[name].at[h, n_kv - 1], lambda n: s[name].at[h, n], s[name].at[h, : n_kv - 1]
+            name, h, devices, lambda p: s[name].at[h, n_kv - 1], lambda n: s[name].at[h, n], s[name].at[h, : n_kv - 1]
         )
 
     def scale_of(name, h, wait):
@@ -401,13 +405,13 @@
     first, second, copies_m, copies_q = [], [], [], []
 
     def project_first(h):
-        normed, squares = normalise(gathered.at[h], s["gain"])
+        normed, s["squares"][h, n_kv - 1] = normalise(gathered.at[h], s["gain"])
         ready("wqk")
         out_a[h] = project(normed, s["wqk"])
+        copies_q.append(send_squares("squares", h, peers))
         first.append(kv_send("a", h, peers, lambda p: out_a.at[h, p], lambda n: in_a.at[h, n], in_a.at[h]))
         ready("wvg")
         out_b[h] = project(normed, s["wvg"])
-        copies_q.append(send_squares("squares", h, squares))
         second.append(kv_send("b", h, peers, lambda p: out_b.at[h, p], lambda n: in_b.at[h, n], in_b.at[h]))
 
     decays = []
@@ -471,30 +475,36 @@
         lax.fori_loop(0, rows // block, update_step, 0)
 
     def reduce_start(h, lhs, weight, tag):
-        start_reduce(lhs, s[weight], s["parts_" + tag].at[h], s["swapped_" + tag].at[h], tp, *pair_of(tag, h))
+        start_reduce(lhs, s[weight], s["parts_" + tag].at[h], s["swapped_" + tag].at[h], tp, *pair_of("x", h))
 
     def reduce_spread(h, tag):
         swapped, staged = s["swapped_" + tag].at[h], s["staged_" + tag].at[h]
-        send_sems, recv_sems = pair_of(tag, h)
+        send_sems, recv_sems = pair_of("x", h)
         spread_pairs(s["parts_" + tag].at[h], swapped, staged, s["landed_" + tag].at[h], tp, send_sems, recv_sems)
         closing.extend([(swapped, send_sems.at[0]), (staged, send_sems.at[1])])
 
     def reduce_total(h, tag):
         into = s["landed_" + tag].at[h]
-        landed(into, pair_of(tag, h)[1].at[1])
+        landed(into, pair_of("x", h)[1].at[1])
         return total_of(into[0], into.at[1:])
 
     gate_out, up_out, gate_in, up_in = s["gate_out"], s["up_out"], s["gate_in"], s["up_in"]
     copies_e, copies_f, copies_h, copies_u = [], [], [], []
     crossed_all = crossed + [beside]
+    first_units = (units // LANES + 1) // 2 * LANES
 
     def project_second(h):
-        normed, squares = normalise(gathered_two.at[h], s["gain_two"])
-        gate_out[h] = project(normed, s["fg"])
-        copies_e.append(
-            kv_send("e", h, crossed_all, lambda p: gate_out.at[h, p], lambda n: gate_in.at[h, n], gate_in.at[h])
-        )
-        copies_u.append(send_squares("squares_two", h, squares))
+        normed, s["squares_two"][h, n_kv - 1] = normalise(gathered_two.at[h], s["gain_two"])
+        for span in (slice(0, first_units), slice(first_units, units)):
+            gate_out[h, :, :, span] = project(normed, s["fg"].at[:, span])
+            if span.start == 0:
+                copies_u.append(send_squares("squares_two", h, crossed))
+            send_all(
+                crossed_all, lambda p: gate_out.at[h, p, :, span], lambda n: gate_in.at[h, n, :, span],
+                sems["a"].at[h, 0], sems["a"].at[h, 1],
+            )
+        closing.append((gate_in.at[h], sems["a"].at[h, 0]))
+        copies_e.append(lambda: landed(gate_in.at[h], sems["a"].at[h, 1]))
         up_out[h] = project(normed, s["fu"])
         copies_f.append(
             kv_send("f", h, crossed_all, lambda p: up_out.at[h, p], lambda n: up_in.at[h, n], up_in.at[h])
@@ -529,14 +539,20 @@
         copies_m[h]()
         reduce_start(h, merged[h].reshape(batch, v_width), "wo", "x")
         reduce_spread(h, "x")
-        update(h)
+        if h + 1 < halves:
+            update(h)
+    for gather in first_gather:
+        gather[2]()
     second_gather = []
     for h in range(halves):
         total = reduce_total(h, "x")
         own = gathered[h, tp].reshape(batch, LANES).astype(jnp.float32)
         gathered_two[h, tp] = (own + total).astype(jnp.bfloat16).reshape(n_kv, rows, LANES)
-        second_gather.append(start_gather(gathered_two.at[h], tp, n_tp, 1, *pair_of("c", h)))
+        second_gather.append(start_gather(gathered_two.at[h], tp, n_tp, 1, *pair_of("g", h)))
+        if h == 0:
+            update(halves - 1)
     ready("gain_two", "fg", "fu")
+    close_sends()
     for h in range(halves):
         second_gather[h][1]()
         second_gather[h][0](0, chips - 1)
@@ -552,9 +568,8 @@
         total = reduce_total(h, "d")
         own = gathered_two[h, tp].reshape(batch, LANES).astype(jnp.float32)
         out[:, h] = (own + total).astype(jnp.bfloat16).reshape(n_kv, rows, LANES)
-    for extent, sem in closing:
-        landed(extent, sem)
-    for gather in first_gather + second_gather:
+    close_sends()
+    for gather in second_gather:
         gather[2]()
 
 
@@ -575,6 +590,7 @@
 
 
 HALVES = 2
+SHARED = {"f": "b", "h": "m", "squares_two": "squares"}
 
 
 def fused_on_device(n_kv, n_tp, *arrays):
@@ -633,11 +649,8 @@
         scratch["landed_" + tag] = buffer(chips, batch, columns)
     dma = pltpu.SemaphoreType.DMA
     sems = {"load": dma((12,))}
-    for tag in ("g", "c"):
-        sems[tag + "_s"], sems[tag + "_r"] = dma((HALVES, 2)), dma((HALVES, n_tp))
-    for tag in ("x", "d"):
-        sems[tag + "_s"] = sems[tag + "_r"] = dma((HALVES, 2))
-    for tag in ("a", "b", "m", "e", "f", "h", "squares", "squares_two"):
+    sems["g_s"], sems["g_r"] = dma((HALVES, 2)), dma((HALVES, n_tp))
+    for tag in ("x_s", "x_r", "a", "b", "m", "squares"):
         sems[tag] = dma((HALVES, 2))
     operands = (
         tokens.reshape(n_kv, HALVES, rows, columns), lengths[None, :], freq, mixer_gain[None, :],

time: 51.7 us -> 50.6 us (0.979)
  Pallas kernels: 50.9 us -> 49.9 us
    pallas_call x1, Pallas kernels: 47.5 us -> 46.5 us  [fused_on_device(): pl.pallas_call(functools.partial(layer_kernel, n_kv, n_tp, depth * n_kv),...]
where the time goes in v4:
time: 50.6 us; the launch traced here: 50.5 us
  Pallas kernels  49.9 us (99%)
  between operations  0.64 us (1%)
    pallas_call x1, Pallas kernels, fused_on_device(): pl.pallas_call(functools.partial(layer_kernel, n_kv, n_tp, depth * n_kv),...  46.5 us
    pallas_call x1, Pallas kernels, fused_on_device(): pl.pallas_call(finish_kernel, out_shape=(jax.ShapeDtypeStruct(state.shape...  3.39 us

profile of v4, /device:TPU:0, one launch (start us, length us, event | category | flops | bytes accessed | tf_op | source)
XLA Modules:
  0.0 50.5 jit_solution(4563618978952169286)
XLA Ops:
  0.6 46.5 %layer.1 = (bf16[4,2,16,128]{3,2,1,0:T(8,128)(2,1)S(1)}, f32[32,2,128,256]{3,2,1,0:T(8,128)S(1)}) custom-call(bf16[4,2,16,128]{3,2,1,0:T(8,128)(2,1)} %bitcast.5, s32[1,32]{1,0:T(1,128)} %bitcast.8, f32[1,128]{1,0:T(1,128)} %constant.4.freq_hbm, f32[1,1024]{1,0:T(1,128)} %bitcast.6, f32[1,1024]{1,0:T(1,128)} %bitcast.7, f32[32,2,128,256]{3,2,1,0:T(8,128)} %state_hbm.1, ...), custom_call_target="tpu_custom_call" | custom-call | tf_op jit(solution)/shard_map/layer/pallas_call | solution.py:660
  47.1 3.4 %finish.1 = (f32[32,2,128,256]{3,2,1,0:T(8,128)}, bf16[4,2,16,128]{3,2,1,0:T(8,128)(2,1)}) custom-call(f32[32,2,128,256]{3,2,1,0:T(8,128)S(1)} %get-tuple-element.6.state, bf16[4,2,16,128]{3,2,1,0:T(8,128)(2,1)S(1)} %get-tuple-element.7.out), custom_call_target="tpu_custom_call" | custom-call | tf_op jit(solution)/shard_map/finish/pallas_call | solution.py:671

commit v5 on v4

--- a/solution.py
+++ b/solution.py
@@ -249,7 +249,7 @@
         def _():
             landed(slots.at[: len(relayed)], send_sems.at[1])
 
-    return take, take_own, close
+    return take, take_own, close, order[::-1]
 
 
 def start_reduce(lhs, weight, parts, swapped, tp, send_sems, recv_sems):
@@ -346,6 +346,7 @@
     crossed = [{"kv": peer, "tp": partner} for peer in kv_peers(kv, n_kv)]
     along = [{"kv": kv, "tp": other * CORES + 1 - core} for other in far_first(chip, chips)]
     beside = {"kv": kv, "tp": partner}
+    crossed_all = crossed + [beside]
     aside = [{"kv": kv, "tp": other * CORES + core} for other in far_first(chip, chips)]
     greet(along + aside + [beside] + peers + crossed)
     closing = []
@@ -388,15 +389,33 @@
     lane = lax.broadcasted_iota(jnp.int32, angles.shape, 1)
     sine = jnp.where(lane < QK // 2, -sine, sine)
 
-    def normalise(slots, gains):
-        x = jnp.concatenate(
-            [slots[j].reshape(batch, slots.shape[3]) for j in range(slots.shape[0])], axis=1
-        ).astype(jnp.float32)
-        squares = jnp.sum(x * x, axis=1, keepdims=True)
-        return (x * gains[...]).astype(jnp.bfloat16), as_row(squares)
-
-    def project(lhs, weight):
-        full = jnp.dot(lhs, weight[...], preferred_element_type=jnp.float32)
+    def gathered_product(gather, slots, gains, weight, between=None):
+        take, take_own, _, near = gather
+        span = CORES * columns
+
+        def chunk(source):
+            at = pl.multiple_of(source * span, span)
+            x = jnp.concatenate(
+                [slots[source * CORES + side].reshape(batch, columns) for side in range(CORES)], axis=1
+            ).astype(jnp.float32)
+            part = (x * gains[:, pl.ds(at, span)]).astype(jnp.bfloat16)
+            s["normed"][:, pl.ds(at, span)] = part
+            product = jnp.dot(part, weight[pl.ds(at, span), :], preferred_element_type=jnp.float32)
+            return product, jnp.sum(x * x, axis=1, keepdims=True)
+
+        take_own()
+        if between is not None:
+            between()
+        product, squares = chunk(chip)
+        for k, source in enumerate(near):
+            take(k, k + 1)
+            more, more_squares = chunk(source)
+            product += more
+            squares += more_squares
+        return product.astype(jnp.bfloat16).reshape(n_kv, rows, product.shape[1]), as_row(squares)
+
+    def project(weight):
+        full = jnp.dot(s["normed"][...], weight[...], preferred_element_type=jnp.float32)
         return full.astype(jnp.bfloat16).reshape(n_kv, rows, full.shape[1])
 
     heads = q_width // QK
@@ -404,14 +423,18 @@
     out_a, out_b, in_a, in_b = s["out_a"], s["out_b"], s["in_a"], s["in_b"]
     first, second, copies_m, copies_q = [], [], [], []
 
+    def start_next_gather(h):
+        if h < halves:
+            first_gather.append(start_gather(gathered.at[h], tp, n_tp, 0, *pair_of("g", h)))
+
     def project_first(h):
-        normed, s["squares"][h, n_kv - 1] = normalise(gathered.at[h], s["gain"])
-        ready("wqk")
-        out_a[h] = project(normed, s["wqk"])
+        out_a[h], s["squares"][h, n_kv - 1] = gathered_product(
+            first_gather[h], gathered.at[h], s["gain"], s["wqk"], lambda: start_next_gather(h + 1)
+        )
+        first.append(kv_send("a", h, peers, lambda p: out_a.at[h, p], lambda n: in_a.at[h, n], in_a.at[h]))
         copies_q.append(send_squares("squares", h, peers))
-        first.append(kv_send("a", h, peers, lambda p: out_a.at[h, p], lambda n: in_a.at[h, n], in_a.at[h]))
         ready("wvg")
-        out_b[h] = project(normed, s["wvg"])
+        out_b[h] = project(s["wvg"])
         second.append(kv_send("b", h, peers, lambda p: out_b.at[h, p], lambda n: in_b.at[h, n], in_b.at[h]))
 
     decays = []
@@ -451,10 +474,10 @@
             span = slice(head * width, (head + 1) * width)
             piece = decays[head] * retained[base : base + rows, span] + overlap * values[:, span]
             pieces.append(piece * lax.rsqrt(jnp.mean(piece * piece, axis=1, keepdims=True) + 1e-06))
-        merged[h, kv] = (jnp.concatenate(pieces, axis=1) * silu(total[:, v_width:])).astype(jnp.bfloat16)
-        copies_m.append(kv_send(
-            "m", h, peers, lambda p: merged.at[h, kv], lambda n: merged.at[h, kv], merged.at[h, : n_kv - 1]
-        ))
+        s["merged_out"][h] = (jnp.concatenate(pieces, axis=1) * silu(total[:, v_width:])).astype(jnp.bfloat16)
+        copies_m.append(
+            kv_send("m", h, crossed_all, lambda p: s["merged_out"].at[h], lambda n: merged.at[h, kv], merged.at[h])
+        )
 
     block = 8
 
@@ -490,22 +513,25 @@
 
     gate_out, up_out, gate_in, up_in = s["gate_out"], s["up_out"], s["gate_in"], s["up_in"]
     copies_e, copies_f, copies_h, copies_u = [], [], [], []
-    crossed_all = crossed + [beside]
     first_units = (units // LANES + 1) // 2 * LANES
 
     def project_second(h):
-        normed, s["squares_two"][h, n_kv - 1] = normalise(gathered_two.at[h], s["gain_two"])
         for span in (slice(0, first_units), slice(first_units, units)):
-            gate_out[h, :, :, span] = project(normed, s["fg"].at[:, span])
             if span.start == 0:
-                copies_u.append(send_squares("squares_two", h, crossed))
+                gate_out[h, :, :, span], s["squares_two"][h, n_kv - 1] = gathered_product(
+                    second_gather[h], gathered_two.at[h], s["gain_two"], s["fg"].at[:, span]
+                )
+            else:
+                gate_out[h, :, :, span] = project(s["fg"].at[:, span])
             send_all(
                 crossed_all, lambda p: gate_out.at[h, p, :, span], lambda n: gate_in.at[h, n, :, span],
                 sems["a"].at[h, 0], sems["a"].at[h, 1],
             )
+            if span.start == 0:
+                copies_u.append(send_squares("squares_two", h, crossed))
         closing.append((gate_in.at[h], sems["a"].at[h, 0]))
         copies_e.append(lambda: landed(gate_in.at[h], sems["a"].at[h, 1]))
-        up_out[h] = project(normed, s["fu"])
+        up_out[h] = project(s["fu"])
         copies_f.append(
             kv_send("f", h, crossed_all, lambda p: up_out.at[h, p], lambda n: up_in.at[h, n], up_in.at[h])
         )
@@ -522,28 +548,25 @@
             kv_send("h", h, crossed_all, lambda p: s["hidden_out"].at[h], lambda n: hidden.at[h, kv], hidden.at[h])
         )
 
-    first_gather[0][0](0, 1)
+    second_gather = []
+    ready("wqk")
+    project_first(0)
+    ready("wo")
+    remote_to(beside, s["wo"], s["wo_far"], sems["wo"].at[0], sems["wo"].at[1]).start()
     for h in range(1, halves):
-        first_gather.append(start_gather(gathered.at[h], tp, n_tp, 0, *pair_of("g", h)))
-    first_gather[0][0](1, chips - 1)
-    for h in range(halves):
-        if h > 0:
-            first_gather[h][0](0, chips - 1)
-        first_gather[h][1]()
         project_first(h)
     ready("state")
     for h in range(halves):
         attend(h)
-    ready("wo")
+    landed(s["wo_far"], sems["wo"].at[1])
     for h in range(halves):
         copies_m[h]()
-        reduce_start(h, merged[h].reshape(batch, v_width), "wo", "x")
+        reduce_start(h, merged[h].reshape(batch, v_width), "wo_far", "x")
         reduce_spread(h, "x")
         if h + 1 < halves:
             update(h)
     for gather in first_gather:
         gather[2]()
-    second_gather = []
     for h in range(halves):
         total = reduce_total(h, "x")
         own = gathered[h, tp].reshape(batch, LANES).astype(jnp.float32)
@@ -552,10 +575,9 @@
         if h == 0:
             update(halves - 1)
     ready("gain_two", "fg", "fu")
+    landed(s["wo_far"], sems["wo"].at[0])
     close_sends()
     for h in range(halves):
-        second_gather[h][1]()
-        second_gather[h][0](0, chips - 1)
         project_second(h)
     for h in range(halves):
         activate(h)
@@ -628,6 +650,8 @@
         "retained": pltpu.VMEM((HALVES * rows, v_width), f32),
         "value": pltpu.VMEM((HALVES * rows, v_width), f32),
         "merged": buffer(n_kv, rows, v_width),
+        "merged_out": buffer(rows, v_width),
+        "normed": pltpu.VMEM((batch, depth), bf16),
         "gate_out": buffer(n_kv, rows, units),
         "up_out": buffer(n_kv, rows, units),
         "gate_in": buffer(n_kv, rows, units),
@@ -639,7 +663,9 @@
     }
     shapes = {
         "wqk": (depth, 2 * q_width), "wvg": (depth, 2 * v_width), "fg": fg.shape, "fu": fu.shape,
-        "wo": (CORES, wo.shape[0], chips * columns), "fd": (CORES, fd.shape[0], chips * columns),
+        "wo": (CORES, wo.shape[0], chips * columns),
+        "wo_far": (CORES, wo.shape[0], chips * columns),
+        "fd": (CORES, fd.shape[0], chips * columns),
     }
     scratch.update({name: pltpu.VMEM(shape, bf16) for name, shape in shapes.items()})
     for tag in ("x", "d"):
@@ -648,7 +674,7 @@
         scratch["staged_" + tag] = buffer(chips, batch, columns)
         scratch["landed_" + tag] = buffer(chips, batch, columns)
     dma = pltpu.SemaphoreType.DMA
-    sems = {"load": dma((12,))}
+    sems = {"load": dma((12,)), "wo": dma((2,))}
     sems["g_s"], sems["g_r"] = dma((HALVES, 2)), dma((HALVES, n_tp))
     for tag in ("x_s", "x_r", "a", "b", "m", "squares"):
         sems[tag] = dma((HALVES, 2))

time: 50.6 us -> 49.9 us (0.986)
  Pallas kernels: 49.9 us -> 49.2 us
    pallas_call x1, Pallas kernels: 46.5 us -> 45.8 us  [fused_on_device(): pl.pallas_call(functools.partial(layer_kernel, n_kv, n_tp, depth * n_kv),...]
where the time goes in v5:
time: 49.9 us; the launch traced here: 49.8 us
  Pallas kernels  49.2 us (99%)
  between operations  0.64 us (1%)
    pallas_call x1, Pallas kernels, fused_on_device(): pl.pallas_call(functools.partial(layer_kernel, n_kv, n_tp, depth * n_kv),...  45.8 us
    pallas_call x1, Pallas kernels, fused_on_device(): pl.pallas_call(finish_kernel, out_shape=(jax.ShapeDtypeStruct(state.shape...  3.39 us

profile of v5, /device:TPU:0, one launch (start us, length us, event | category | flops | bytes accessed | tf_op | source)
XLA Modules:
  0.0 49.8 jit_solution(6113096256234257186)
XLA Ops:
  0.6 45.8 %layer.1 = (bf16[4,2,16,128]{3,2,1,0:T(8,128)(2,1)S(1)}, f32[32,2,128,256]{3,2,1,0:T(8,128)S(1)}) custom-call(bf16[4,2,16,128]{3,2,1,0:T(8,128)(2,1)} %bitcast.5, s32[1,32]{1,0:T(1,128)} %bitcast.8, f32[1,128]{1,0:T(1,128)} %constant.4.freq_hbm, f32[1,1024]{1,0:T(1,128)} %bitcast.6, f32[1,1024]{1,0:T(1,128)} %bitcast.7, f32[32,2,128,256]{3,2,1,0:T(8,128)} %state_hbm.1, ...), custom_call_target="tpu_custom_call" | custom-call | tf_op jit(solution)/shard_map/layer/pallas_call | solution.py:686
  46.4 3.4 %finish.1 = (f32[32,2,128,256]{3,2,1,0:T(8,128)}, bf16[4,2,16,128]{3,2,1,0:T(8,128)(2,1)}) custom-call(f32[32,2,128,256]{3,2,1,0:T(8,128)S(1)} %get-tuple-element.6.state, bf16[4,2,16,128]{3,2,1,0:T(8,128)(2,1)S(1)} %get-tuple-element.7.out), custom_call_target="tpu_custom_call" | custom-call | tf_op jit(solution)/shard_map/finish/pallas_call | solution.py:697

commit v6 on v5

--- a/solution.py
+++ b/solution.py
@@ -317,8 +317,12 @@
         "lengths": [(lengths_hbm, s["lengths"])],
         "freq": [(freq_hbm, s["freq"])],
         "gain": [(gain_hbm, s["gain"])],
-        "wqk": [(wq_hbm, s["wqk"].at[:, :q_width]), (wk_hbm, s["wqk"].at[:, q_width:])],
-        "wvg": [(wv_hbm, s["wvg"].at[:, :v_width]), (wg_hbm, s["wvg"].at[:, v_width:])],
+        "wp": [
+            (wq_hbm, s["wp"].at[:, :q_width]),
+            (wk_hbm, s["wp"].at[:, q_width : 2 * q_width]),
+            (wv_hbm, s["wp"].at[:, 2 * q_width : 2 * q_width + v_width]),
+            (wg_hbm, s["wp"].at[:, 2 * q_width + v_width :]),
+        ],
         "state": [(state_hbm, state)],
         "wo": sides(wo_hbm, s["wo"]),
         "gain_two": [(gain_two_hbm, s["gain_two"])],
@@ -327,7 +331,7 @@
         "fd": sides(fd_hbm, s["fd"]),
     }
     wholes = {
-        "tokens": gathered.at[:, tp], "wqk": s["wqk"], "wvg": s["wvg"], "state": state, "wo": s["wo"], "fd": s["fd"],
+        "tokens": gathered.at[:, tp], "wp": s["wp"], "state": state, "wo": s["wo"], "fd": s["fd"],
         "lengths": s["lengths"], "freq": s["freq"], "gain": s["gain"],
         "gain_two": s["gain_two"], "fg": s["fg"], "fu": s["fu"],
     }
@@ -380,15 +384,6 @@
     ready("tokens")
     first_gather = [start_gather(gathered.at[0], tp, n_tp, 0, *pair_of("g", 0))]
     ready("lengths", "freq", "gain")
-    all_rows = halves * rows
-    row = lax.broadcasted_iota(jnp.int32, (all_rows, all_rows), 0)
-    col = lax.broadcasted_iota(jnp.int32, (all_rows, all_rows), 1)
-    spread = jnp.where(row == col, s["lengths"][...].astype(jnp.float32), 0.0)
-    angles = jnp.sum(spread, axis=1, keepdims=True) * s["freq"][...]
-    cosine, sine = jnp.cos(angles), jnp.sin(angles)
-    lane = lax.broadcasted_iota(jnp.int32, angles.shape, 1)
-    sine = jnp.where(lane < QK // 2, -sine, sine)
-
     def gathered_product(gather, slots, gains, weight, between=None):
         take, take_own, _, near = gather
         span = CORES * columns
@@ -404,9 +399,9 @@
             return product, jnp.sum(x * x, axis=1, keepdims=True)
 
         take_own()
+        product, squares = chunk(chip)
         if between is not None:
             between()
-        product, squares = chunk(chip)
         for k, source in enumerate(near):
             take(k, k + 1)
             more, more_squares = chunk(source)
@@ -423,18 +418,33 @@
     out_a, out_b, in_a, in_b = s["out_a"], s["out_b"], s["in_a"], s["in_b"]
     first, second, copies_m, copies_q = [], [], [], []
 
+    angles_of = []
+
+    def find_angles():
+        all_rows = halves * rows
+        row = lax.broadcasted_iota(jnp.int32, (all_rows, all_rows), 0)
+        col = lax.broadcasted_iota(jnp.int32, (all_rows, all_rows), 1)
+        spread = jnp.where(row == col, s["lengths"][...].astype(jnp.float32), 0.0)
+        angles = jnp.sum(spread, axis=1, keepdims=True) * s["freq"][...]
+        cosine, sine = jnp.cos(angles), jnp.sin(angles)
+        lane = lax.broadcasted_iota(jnp.int32, angles.shape, 1)
+        sine = jnp.where(lane < QK // 2, -sine, sine)
+        angles_of.extend([cosine, sine])
+
     def start_next_gather(h):
+        if h == 1:
+            find_angles()
         if h < halves:
             first_gather.append(start_gather(gathered.at[h], tp, n_tp, 0, *pair_of("g", h)))
 
     def project_first(h):
-        out_a[h], s["squares"][h, n_kv - 1] = gathered_product(
-            first_gather[h], gathered.at[h], s["gain"], s["wqk"], lambda: start_next_gather(h + 1)
+        product, s["squares"][h, n_kv - 1] = gathered_product(
+            first_gather[h], gathered.at[h], s["gain"], s["wp"], lambda: start_next_gather(h + 1)
         )
+        out_a[h] = product[:, :, : 2 * q_width]
+        out_b[h] = product[:, :, 2 * q_width :]
         first.append(kv_send("a", h, peers, lambda p: out_a.at[h, p], lambda n: in_a.at[h, n], in_a.at[h]))
         copies_q.append(send_squares("squares", h, peers))
-        ready("wvg")
-        out_b[h] = project(s["wvg"])
         second.append(kv_send("b", h, peers, lambda p: out_b.at[h, p], lambda n: in_b.at[h, n], in_b.at[h]))
 
     decays = []
@@ -449,7 +459,7 @@
         total = total_of(out_a[h, kv], in_a.at[h])
         scale = scale_of("squares", h, copies_q[h])
         total = total * scale
-        cosines, sines = cosine[base : base + rows], sine[base : base + rows]
+        cosines, sines = [table[base : base + rows] for table in angles_of]
         blocks = []
         for start, factor in ((0, 1.0), (q_width, QK ** (-0.5))):
             for head in range(heads):
@@ -549,7 +559,7 @@
         )
 
     second_gather = []
-    ready("wqk")
+    ready("wp")
     project_first(0)
     ready("wo")
     remote_to(beside, s["wo"], s["wo_far"], sems["wo"].at[0], sems["wo"].at[1]).start()
@@ -595,23 +605,18 @@
         gather[2]()
 
 
-def finish_kernel(state, out, state_to, out_to, store_sems):
-    chunks = store_sems.shape[0] - 1
+def finish_kernel(chunks, state, out, state_to, out_to, sems):
     size = state.shape[0] // chunks
-    targets = [(out, out_to)]
     for i in range(chunks):
         part = pl.ds(i * size, size)
-        targets.append((state.at[part], state_to.at[part]))
-    copies = [
-        pltpu.make_async_copy(source, target, store_sems.at[i]) for i, (source, target) in enumerate(targets)
-    ]
-    for copy in copies:
-        copy.start()
-    for copy in copies:
-        copy.wait()
+        pltpu.make_async_copy(state.at[part], state_to.at[part], sems.at[0]).start()
+    pltpu.make_async_copy(out, out_to, sems.at[1]).start()
+    pltpu.make_async_copy(state, state_to, sems.at[0]).wait()
+    pltpu.make_async_copy(out, out_to, sems.at[1]).wait()
 
 
 HALVES = 2
+FINISH_CHUNKS = 8
 SHARED = {"f": "b", "h": "m", "squares_two": "squares"}
 
 
@@ -662,7 +667,7 @@
         "squares_two": buffer(n_kv, 1, LANES, dtype=f32),
     }
     shapes = {
-        "wqk": (depth, 2 * q_width), "wvg": (depth, 2 * v_width), "fg": fg.shape, "fu": fu.shape,
+        "wp": (depth, 2 * q_width + 2 * v_width), "fg": fg.shape, "fu": fu.shape,
         "wo": (CORES, wo.shape[0], chips * columns),
         "wo_far": (CORES, wo.shape[0], chips * columns),
         "fd": (CORES, fd.shape[0], chips * columns),
@@ -674,7 +679,7 @@
         scratch["staged_" + tag] = buffer(chips, batch, columns)
         scratch["landed_" + tag] = buffer(chips, batch, columns)
     dma = pltpu.SemaphoreType.DMA
-    sems = {"load": dma((12,)), "wo": dma((2,))}
+    sems = {"load": dma((11,)), "wo": dma((2,))}
     sems["g_s"], sems["g_r"] = dma((HALVES, 2)), dma((HALVES, n_tp))
     for tag in ("x_s", "x_r", "a", "b", "m", "squares"):
         sems[tag] = dma((HALVES, 2))
@@ -695,14 +700,14 @@
         name="layer",
     )(*[pltpu.with_memory_space_constraint(a, pltpu.HBM) for a in operands])
     new_state, out = pl.pallas_call(
-        finish_kernel,
+        functools.partial(finish_kernel, FINISH_CHUNKS),
         out_shape=(
             jax.ShapeDtypeStruct(state.shape, f32),
             jax.ShapeDtypeStruct(out_shape, bf16),
         ),
         in_specs=[vmem, vmem],
         out_specs=(hbm, hbm),
-        scratch_shapes=[pltpu.SemaphoreType.DMA((9,))],
+        scratch_shapes=[dma((2,))],
         compiler_params=pltpu.CompilerParams(vmem_limit_bytes=FINISH_VMEM),
         name="finish",
     )(new_state, out)

time: 49.9 us -> 49.5 us (level)
  Pallas kernels: 49.2 us -> 48.7 us
where the time goes in v6:
time: 49.5 us; the launch traced here: 49.3 us
  Pallas kernels  48.7 us (98%)
  between operations  0.64 us (1%)
    pallas_call x1, Pallas kernels, fused_on_device(): pl.pallas_call(functools.partial(layer_kernel, n_kv, n_tp, depth * n_kv),...  45.4 us
    pallas_call x1, Pallas kernels, fused_on_device(): pl.pallas_call(functools.partial(finish_kernel, FINISH_CHUNKS), out_shape...  3.32 us

profile of v6, /device:TPU:0, one launch (start us, length us, event | category | flops | bytes accessed | tf_op | source)
XLA Modules:
  0.0 49.3 jit_solution(14318245025593972688)
XLA Ops:
  0.6 45.4 %layer.1 = (bf16[4,2,16,128]{3,2,1,0:T(8,128)(2,1)S(1)}, f32[32,2,128,256]{3,2,1,0:T(8,128)S(1)}) custom-call(bf16[4,2,16,128]{3,2,1,0:T(8,128)(2,1)} %bitcast.5, s32[1,32]{1,0:T(1,128)} %bitcast.8, f32[1,128]{1,0:T(1,128)} %constant.4.freq_hbm, f32[1,1024]{1,0:T(1,128)} %bitcast.6, f32[1,1024]{1,0:T(1,128)} %bitcast.7, f32[32,2,128,256]{3,2,1,0:T(8,128)} %state_hbm.1, ...), custom_call_target="tpu_custom_call" | custom-call | tf_op jit(solution)/shard_map/layer/pallas_call | solution.py:691
  46.0 3.3 %finish.1 = (f32[32,2,128,256]{3,2,1,0:T(8,128)}, bf16[4,2,16,128]{3,2,1,0:T(8,128)(2,1)}) custom-call(f32[32,2,128,256]{3,2,1,0:T(8,128)S(1)} %get-tuple-element.6.state, bf16[4,2,16,128]{3,2,1,0:T(8,128)(2,1)S(1)} %get-tuple-element.7.out), custom_call_target="tpu_custom_call" | custom-call | tf_op jit(solution)/shard_map/finish/pallas_call | solution.py:702

commit v7 on v6

--- a/solution.py
+++ b/solution.py
@@ -573,8 +573,8 @@
         copies_m[h]()
         reduce_start(h, merged[h].reshape(batch, v_width), "wo_far", "x")
         reduce_spread(h, "x")
-        if h + 1 < halves:
-            update(h)
+    for h in range(halves - 1):
+        update(h)
     for gather in first_gather:
         gather[2]()
     for h in range(halves):
@@ -616,7 +616,7 @@
 
 
 HALVES = 2
-FINISH_CHUNKS = 8
+FINISH_CHUNKS = 16
 SHARED = {"f": "b", "h": "m", "squares_two": "squares"}
 
 

time: 49.5 us -> 49.3 us (level)
  no operation moved by 1% of the time
where the time goes in v7:
time: 49.3 us; the launch traced here: 49.2 us
  Pallas kernels  48.6 us (99%)
  between operations  0.64 us (1%)
    pallas_call x1, Pallas kernels, fused_on_device(): pl.pallas_call(functools.partial(layer_kernel, n_kv, n_tp, depth * n_kv),...  45.3 us
    pallas_call x1, Pallas kernels, fused_on_device(): pl.pallas_call(functools.partial(finish_kernel, FINISH_CHUNKS), out_shape...  3.29 us

profile of v7, /device:TPU:0, one launch (start us, length us, event | category | flops | bytes accessed | tf_op | source)
XLA Modules:
  0.0 49.2 jit_solution(3070826106446145067)
XLA Ops:
  0.6 45.3 %layer.1 = (bf16[4,2,16,128]{3,2,1,0:T(8,128)(2,1)S(1)}, f32[32,2,128,256]{3,2,1,0:T(8,128)S(1)}) custom-call(bf16[4,2,16,128]{3,2,1,0:T(8,128)(2,1)} %bitcast.5, s32[1,32]{1,0:T(1,128)} %bitcast.8, f32[1,128]{1,0:T(1,128)} %constant.4.freq_hbm, f32[1,1024]{1,0:T(1,128)} %bitcast.6, f32[1,1024]{1,0:T(1,128)} %bitcast.7, f32[32,2,128,256]{3,2,1,0:T(8,128)} %state_hbm.1, ...), custom_call_target="tpu_custom_call" | custom-call | tf_op jit(solution)/shard_map/layer/pallas_call | solution.py:691
  45.9 3.3 %finish.1 = (f32[32,2,128,256]{3,2,1,0:T(8,128)}, bf16[4,2,16,128]{3,2,1,0:T(8,128)(2,1)}) custom-call(f32[32,2,128,256]{3,2,1,0:T(8,128)S(1)} %get-tuple-element.6.state, bf16[4,2,16,128]{3,2,1,0:T(8,128)(2,1)S(1)} %get-tuple-element.7.out), custom_call_target="tpu_custom_call" | custom-call | tf_op jit(solution)/shard_map/finish/pallas_call | solution.py:702

commit v8 on v7

--- a/solution.py
+++ b/solution.py
@@ -523,10 +523,10 @@
 
     gate_out, up_out, gate_in, up_in = s["gate_out"], s["up_out"], s["gate_in"], s["up_in"]
     copies_e, copies_f, copies_h, copies_u = [], [], [], []
-    first_units = (units // LANES + 1) // 2 * LANES
+    first_units = units
 
     def project_second(h):
-        for span in (slice(0, first_units), slice(first_units, units)):
+        for span in (slice(0, first_units),):
             if span.start == 0:
                 gate_out[h, :, :, span], s["squares_two"][h, n_kv - 1] = gathered_product(
                     second_gather[h], gathered_two.at[h], s["gain_two"], s["fg"].at[:, span]

time: 49.3 us -> 49.1 us (level)
  no operation moved by 1% of the time
where the time goes in v8:
time: 49.1 us; the launch traced here: 49 us
  Pallas kernels  48.3 us (98%)
  between operations  0.64 us (1%)
    pallas_call x1, Pallas kernels, fused_on_device(): pl.pallas_call(functools.partial(layer_kernel, n_kv, n_tp, depth * n_kv),...  45.1 us
    pallas_call x1, Pallas kernels, fused_on_device(): pl.pallas_call(functools.partial(finish_kernel, FINISH_CHUNKS), out_shape...  3.29 us

profile of v8, /device:TPU:0, one launch (start us, length us, event | category | flops | bytes accessed | tf_op | source)
XLA Modules:
  0.0 49.0 jit_solution(12957729648415293738)
XLA Ops:
  0.6 45.1 %layer.1 = (bf16[4,2,16,128]{3,2,1,0:T(8,128)(2,1)S(1)}, f32[32,2,128,256]{3,2,1,0:T(8,128)S(1)}) custom-call(bf16[4,2,16,128]{3,2,1,0:T(8,128)(2,1)} %bitcast.5, s32[1,32]{1,0:T(1,128)} %bitcast.8, f32[1,128]{1,0:T(1,128)} %constant.4.freq_hbm, f32[1,1024]{1,0:T(1,128)} %bitcast.6, f32[1,1024]{1,0:T(1,128)} %bitcast.7, f32[32,2,128,256]{3,2,1,0:T(8,128)} %state_hbm.1, ...), custom_call_target="tpu_custom_call" | custom-call | tf_op jit(solution)/shard_map/layer/pallas_call | solution.py:691
  45.7 3.3 %finish.1 = (f32[32,2,128,256]{3,2,1,0:T(8,128)}, bf16[4,2,16,128]{3,2,1,0:T(8,128)(2,1)}) custom-call(f32[32,2,128,256]{3,2,1,0:T(8,128)S(1)} %get-tuple-element.6.state, bf16[4,2,16,128]{3,2,1,0:T(8,128)(2,1)S(1)} %get-tuple-element.7.out), custom_call_target="tpu_custom_call" | custom-call | tf_op jit(solution)/shard_map/finish/pallas_call | solution.py:702
